TPU v7x, 512 devices: a whole 4x4x16 slice. The times are simulated.
512 devices in a mesh: row: 16 (over y, x), col: 32 (over z, core).
Axes of the slice: x: 4, y: 4, z: 16, core: 2. Of those that a mesh axis runs over, the one named last changes fastest.
Arguments:
- mix_input: bfloat16 [4, 65536, 512], P(None, ('row', 'col')), may hold values from -6 to 6
- group_maps: bfloat16 [4, 128, 128], replicated, may hold values from -0.5 to 0.5
- out_map: bfloat16 [512, 2048], replicated, may hold values from -0.25 to 0.25
Outputs:
- mixed: bfloat16 [4, 65536, 2048], P(None, ('row', 'col'))
All inputs are finite; a program needn't handle non-finite values.
Results may differ from a plain program's by a relative error of at most 0.011.
Values may be sent and summed in bfloat16 or wider, within the bound.
A program may use at most 64 MiB of HBM per device.

v0:
```python
import math

import jax
import jax.numpy as jnp
from jax import lax
from jax.sharding import PartitionSpec as P

precise = lax.Precision.HIGHEST


def angle_pair(left_ids, right_ids, modulus):
    turn_count = left_ids[:, None] * right_ids[None, :] % modulus
    angles = turn_count.astype(jnp.float32) * (2.0 * math.pi / modulus)
    return (jnp.cos(angles), jnp.sin(angles))


def rotate(real_part, imag_part, cosine, sine_part):
    return (real_part * cosine + imag_part * sine_part, imag_part * cosine - real_part * sine_part)


def transform(real_in, imag_in, cosine, sine_part, einsum_form):
    real_out = jnp.einsum(einsum_form, real_in, cosine, precision=precise) + jnp.einsum(
        einsum_form, imag_in, sine_part, precision=precise
    )
    imag_out = jnp.einsum(einsum_form, imag_in, cosine, precision=precise) - jnp.einsum(
        einsum_form, real_in, sine_part, precision=precise
    )
    return (real_out, imag_out)


def per_device(mix_input, group_maps, out_map):
    sequences, positions, channels = mix_input.shape
    group_count, group_width, _ = group_maps.shape
    row_count = lax.axis_size("row")
    col_count = lax.axis_size("col")
    row_id = lax.axis_index("row")
    col_id = lax.axis_index("col")
    block_span = col_count * positions
    length = row_count * block_span
    norm_factor = 1.0 / math.sqrt(length * group_width)
    width_ids = jnp.arange(group_width, dtype=jnp.int32)
    real_tab, sine_tab = angle_pair(width_ids, width_ids, group_width)
    imag_tab = -sine_tab
    lane_count = real_tab.shape[1]
    signal = mix_input.astype(jnp.float32).reshape(sequences, positions, group_count, group_width)
    real_part = jnp.einsum("spgj,jl->sglp", signal, real_tab, precision=precise)
    imag_part = jnp.einsum("spgj,jl->sglp", signal, imag_tab, precision=precise)
    total_items = sequences * group_count * lane_count
    row_items = total_items // row_count
    dev_items = row_items // col_count
    send_shape = (row_count, row_items, 1, positions)
    col_shape = (col_count, dev_items, row_count, 1, positions)
    row_ids = jnp.arange(row_count, dtype=jnp.int32)
    pos_ids = jnp.arange(positions, dtype=jnp.int32)
    col_ids = jnp.arange(col_count, dtype=jnp.int32)
    row_cos, row_sin = angle_pair(row_ids, row_ids, row_count)
    turn_cos, turn_sin = angle_pair(row_ids, col_id * positions + pos_ids, length)
    col_cos, col_sin = angle_pair(col_ids, col_ids, col_count)
    step_cos, step_sin = angle_pair(col_ids, pos_ids, block_span)
    pos_cos, pos_sin = angle_pair(pos_ids, pos_ids, positions)
    row_send = (real_part.reshape(send_shape), imag_part.reshape(send_shape))
    pieces = (
        lax.all_to_all(
            row_send[0].astype(jnp.bfloat16), "row", split_axis=0, concat_axis=2, tiled=True
        ).astype(jnp.float32),
        lax.all_to_all(
            row_send[1].astype(jnp.bfloat16), "row", split_axis=0, concat_axis=2, tiled=True
        ).astype(jnp.float32),
    )
    spun_pair = transform(pieces[0][0], pieces[1][0], row_cos, row_sin, "nrp,rk->nkp")
    real_out, imag_out = rotate(spun_pair[0], spun_pair[1], turn_cos, turn_sin)
    real_rows = real_out[None]
    imag_rows = imag_out[None]
    pieces = (
        lax.all_to_all(
            real_rows.reshape(col_shape), "col", split_axis=0, concat_axis=3, tiled=True
        ),
        lax.all_to_all(
            imag_rows.reshape(col_shape), "col", split_axis=0, concat_axis=3, tiled=True
        ),
    )
    spun_pair = transform(pieces[0][0], pieces[1][0], col_cos, col_sin, "nacp,cb->nabp")
    turned = rotate(spun_pair[0], spun_pair[1], step_cos, step_sin)
    real_out = jnp.einsum("nabp,pq->nqba", turned[0], pos_cos, precision=precise) + jnp.einsum(
        "nabp,pq->nqba", turned[1], pos_sin, precision=precise
    )
    real_spec = real_out.reshape(1, real_out.shape[0], length)
    spectrum = real_spec[0][:, None]
    spectrum = (spectrum * norm_factor).astype(jnp.bfloat16)
    halves = spectrum.shape[1]
    spectrum = spectrum.reshape(1, dev_items, halves, row_count, col_count, positions)
    returned = lax.all_to_all(spectrum, "col", split_axis=4, concat_axis=0, tiled=True)
    held_groups = sequences * group_count // row_count
    returned = returned.reshape(held_groups, lane_count, halves, row_count, positions)
    full_width = returned[:, :, 0]
    group_ids = (row_id * held_groups + jnp.arange(held_groups, dtype=jnp.int32)) % group_count
    picker = (group_ids[:, None] == jnp.arange(group_count, dtype=jnp.int32)[None, :]).astype(
        jnp.bfloat16
    )
    chosen = jnp.einsum(
        "hg,glm->hlm", picker, group_maps, preferred_element_type=jnp.float32
    ).astype(jnp.bfloat16)
    grouped = jnp.einsum(
        "hlap,hlm->hapm", full_width, chosen, preferred_element_type=jnp.float32
    ).astype(jnp.bfloat16)
    grouped = grouped.reshape(1, held_groups, row_count, positions, group_width)
    arrived = lax.all_to_all(grouped, "row", split_axis=2, concat_axis=0, tiled=True)
    arrived = arrived.reshape(sequences, group_count, positions, group_width)
    mixed_out = jnp.einsum(
        "sgpm,gmn->spn",
        arrived,
        out_map.reshape(group_count, group_width, out_map.shape[1]),
        preferred_element_type=jnp.float32,
    )
    return mixed_out.astype(jnp.bfloat16)


def solution(mesh):
    return jax.shard_map(
        per_device,
        mesh=mesh,
        in_specs=(P(None, ("row", "col"), None), P(), P()),
        out_specs=P(None, ("row", "col"), None),
        check_vma=False,
    )
```

profile of v0, /device:TPU:1, one launch (start us, length us, event | category | flops | bytes accessed | tf_op | source)
XLA Modules:
  0.0 248.9 jit_solution(10785886585991419365)
XLA Ops:
  0.0 0.0 copy-start
  0.0 0.0 copy-start.3
  0.0 2.8 %convolution_convert_fusion.2 = bf16[128,4,128,4]{2,0,3,1:T(8,128)(2,1)} fusion(bf16[4,128,512]{2,1,0:T(8,128)(2,1)} %param.3), kind=kOutput, calls=%fused_computation.10 | convolution fusion | flops 403144704 | bytes 1048576 | tf_op jit(solution)/shard_map/spgj,jl->sglp/dot_general | solution.py:46
  2.8 7.6 %all-to-all-start = ((bf16[16,128,1,128]{3,1,2,0:T(8,128)(2,1)}), bf16[16,128,1,128]{3,1,2,0:T(8,128)(2,1)S(1)}, u32[]{:S(2)}, u32[]{:S(2)}) async-start(bf16[16,128,1,128]{3,1,2,0:T(8,128)(2,1)} %bitcast.155), calls=%async_computation | async-start | bytes 1048576 | tf_op jit(solution)/shard_map/all_to_all | solution.py:63
  10.4 0.0 copy-done.3
  10.4 1.6 convolution_convert_fusion.1
  12.1 7.4 %all-to-all-done = bf16[16,128,1,128]{3,1,2,0:T(8,128)(2,1)S(1)} async-done(((bf16[16,128,1,128]{3,1,2,0:T(8,128)(2,1)}), bf16[16,128,1,128]{3,1,2,0:T(8,128)(2,1)S(1)}, u32[]{:S(2)}, u32[]{:S(2)}) %all-to-all-start) | async-done | bytes 524320 | tf_op jit(solution)/shard_map/all_to_all | solution.py:63
  19.5 3.6 %all-to-all-start.1 = ((bf16[16,128,1,128]{3,1,2,0:T(8,128)(2,1)}), bf16[16,128,1,128]{3,1,2,0:T(8,128)(2,1)S(1)}, u32[]{:S(2)}, u32[]{:S(2)}) async-start(bf16[16,128,1,128]{3,1,2,0:T(8,128)(2,1)} %bitcast.154), calls=%async_computation.1 | async-start | bytes 1048576 | tf_op jit(solution)/shard_map/all_to_all | solution.py:66
  23.1 0.1 fusion.104
  23.1 1.7 fusion.26
  24.8 7.4 %all-to-all-done.1 = bf16[16,128,1,128]{3,1,2,0:T(8,128)(2,1)S(1)} async-done(((bf16[16,128,1,128]{3,1,2,0:T(8,128)(2,1)}), bf16[16,128,1,128]{3,1,2,0:T(8,128)(2,1)S(1)}, u32[]{:S(2)}, u32[]{:S(2)}) %all-to-all-start.1) | async-done | bytes 524320 | tf_op jit(solution)/shard_map/all_to_all | solution.py:66
  32.3 0.0 copy-start.2
  32.3 0.7 fusion.28
  33.0 0.5 copy-done.2
  33.5 0.8 convolution_add_fusion.2
  34.3 1.9 multiply_add_fusion
  36.2 75.4 %all_to_all.84 = f32[32,4,16,1,128]{4,2,1,3,0:T(8,128)S(1)} all-to-all(f32[32,4,16,1,128]{4,2,1,3,0:T(8,128)S(1)} %bitcast.152), channel_id=1, replica_groups=mesh['row'=16,'col'=32] {'col'}, dimensions={0} | all-to-all | bytes 2097152 | tf_op jit(solution)/shard_map/all_to_all | solution.py:75
  111.5 4.8 %all-to-all-start.3 = ((f32[32,4,16,1,128]{4,2,1,3,0:T(8,128)}), f32[32,4,16,1,128]{4,2,1,3,0:T(8,128)}, u32[]{:S(2)}, u32[]{:S(2)}) async-start(f32[32,4,16,1,128]{4,2,1,3,0:T(8,128)} %bitcast.151), calls=%async_computation.3 | async-start | bytes 2097152 | tf_op jit(solution)/shard_map/all_to_all | solution.py:78
  116.3 0.1 fusion.89
  116.4 2.6 %fusion.8 = f32[32,4,16,128]{3,0,2,1:T(8,128)} fusion(f32[32,4,16,1,128]{4,2,1,3,0:T(8,128)S(1)} %all_to_all.84), kind=kOutput, calls=%fused_computation.17 | convolution fusion | flops 100677632 | bytes 2097152 | tf_op jit(solution)/shard_map/nacp,cb->nabp/dot_general | solution.py:22
  119.0 53.1 %all-to-all-done.3 = f32[32,4,16,1,128]{4,2,1,3,0:T(8,128)} async-done(((f32[32,4,16,1,128]{4,2,1,3,0:T(8,128)}), f32[32,4,16,1,128]{4,2,1,3,0:T(8,128)}, u32[]{:S(2)}, u32[]{:S(2)}) %all-to-all-start.3) | async-done | bytes 1048608 | tf_op jit(solution)/shard_map/all_to_all | solution.py:78
  172.2 0.0 copy-start.1
  172.2 2.9 %fusion.10 = f32[32,4,16,128]{3,0,2,1:T(8,128)S(1)} fusion(f32[32,4,16,1,128]{4,2,1,3,0:T(8,128)} %all-to-all-done.3), kind=kOutput, calls=%fused_computation.19 | convolution fusion | flops 100677632 | bytes 2097152 | tf_op jit(solution)/shard_map/nacp,cb->nabp/dot_general | solution.py:25
  175.1 0.0 copy-done.1
  175.1 2.8 %convolution_add_fusion.1 = f32[32,4,16,128]{3,0,2,1:T(8,128)S(1)} fusion(f32[32,4,16,128]{3,0,2,1:T(8,128)S(1)} %copy-done.1, f32[32,4,16,1,128]{4,2,1,3,0:T(8,128)} %all-to-all-done.3), kind=kOutput, calls=%fused_computation.4 | convolution fusion | flops 100939776 | bytes 3145728 | tf_op jit(solution)/shard_map/nacp,cb->nabp/dot_general | solution.py:22
  177.9 1.6 convolution_subtract_fusion
  179.5 1.2 fusion.5
  180.7 1.2 fusion.3
  182.0 6.5 %copy.35 = bf16[4,128,32,16]{3,2,1,0:T(8,128)(2,1)} copy(bf16[4,128,32,16]{1,2,3,0:T(8,128)(2,1)S(1)} %fusion.3) | data formatting | bytes 1048576 | tf_op jit(solution)/shard_map/convert_element_type | solution.py:89
  188.5 5.1 %convert_element_type.134 = bf16[1,4,1,16,32,128]{5,4,3,1,2,0:T(8,128)(2,1)S(1)} reshape(bf16[4,128,32,16]{3,2,1,0:T(8,128)(2,1)} %copy.35) | data formatting | bytes 1048576 | tf_op jit(solution)/shard_map/convert_element_type | solution.py:89
  193.6 0.0 copy-start.4
  193.6 1.0 copy.36
  194.6 4.6 %all-to-all-start.4 = ((bf16[1,4,1,16,32,128]{5,3,1,2,0,4:T(8,128)(2,1)}), bf16[1,4,1,16,32,128]{5,3,1,2,0,4:T(8,128)(2,1)S(1)}, u32[]{:S(2)}, u32[]{:S(2)}) async-start(bf16[1,4,1,16,32,128]{5,3,1,2,0,4:T(8,128)(2,1)} %copy.36), calls=%async_computation.4 | async-start | bytes 1048576 | tf_op jit(solution)/shard_map/all_to_all | solution.py:92
  199.2 0.0 copy-done.4
  199.2 0.2 fusion.42
  199.4 33.3 %all-to-all-done.4 = bf16[1,4,1,16,32,128]{5,3,1,2,0,4:T(8,128)(2,1)S(1)} async-done(((bf16[1,4,1,16,32,128]{5,3,1,2,0,4:T(8,128)(2,1)}), bf16[1,4,1,16,32,128]{5,3,1,2,0,4:T(8,128)(2,1)S(1)}, u32[]{:S(2)}, u32[]{:S(2)}) %all-to-all-start.4) | async-done | bytes 524320 | tf_op jit(solution)/shard_map/all_to_all | solution.py:92
  232.7 0.3 fusion.2
  233.0 13.2 %all_to_all.85 = bf16[1,1,16,128,128]{4,3,1,0,2:T(8,128)(2,1)S(1)} all-to-all(bf16[1,1,16,128,128]{4,3,1,0,2:T(8,128)(2,1)S(1)} %fusion.2), channel_id=1, replica_groups=mesh['row'=16,'col'=32] {'row'}, dimensions={2} | all-to-all | bytes 1048576 | tf_op jit(solution)/shard_map/all_to_all | solution.py:107
  246.3 0.0 copy-done
  246.3 2.6 %bitcast_convert_fusion = bf16[4,128,2048]{2,1,0:T(8,128)(2,1)} fusion(bf16[4,4,128,128]{3,2,1,0:T(8,128)(2,1)S(1)} %bitcast.156, bf16[4,128,2048,1]{2,1,0,3:T(8,128)(2,1)S(1)} %bitcast.150), kind=kOutput, calls=%fused_computation | convolution fusion | flops 1074790400 | bytes 4718592 | tf_op jit(solution)/shard_map/sgpm,gmn->spn/dot_general | solution.py:109
  (1 shorter events, 0.0 us)
Async XLA Ops:
  0.0 246.3 %copy-start = (bf16[512,2048]{1,0:T(8,128)(2,1)S(1)}, bf16[512,2048]{1,0:T(8,128)(2,1)}, u32[]{:S(2)}) copy-start(bf16[512,2048]{1,0:T(8,128)(2,1)} %param.5) | copy-start | bytes 6291460
  0.0 10.4 %copy-start.3 = (bf16[4,128,512]{2,1,0:T(8,128)(2,1)S(1)}, bf16[4,128,512]{2,1,0:T(8,128)(2,1)}, u32[]{:S(2)}) copy-start(bf16[4,128,512]{2,1,0:T(8,128)(2,1)} %param.3) | copy-start | bytes 1572868
  2.8 16.6 %all-to-all-start = ((bf16[16,128,1,128]{3,1,2,0:T(8,128)(2,1)}), bf16[16,128,1,128]{3,1,2,0:T(8,128)(2,1)S(1)}, u32[]{:S(2)}, u32[]{:S(2)}) async-start(bf16[16,128,1,128]{3,1,2,0:T(8,128)(2,1)} %bitcast.155), calls=%async_computation | async-start | bytes 1048576 | tf_op jit(solution)/shard_map/all_to_all | solution.py:63
  19.5 12.8 %all-to-all-start.1 = ((bf16[16,128,1,128]{3,1,2,0:T(8,128)(2,1)}), bf16[16,128,1,128]{3,1,2,0:T(8,128)(2,1)S(1)}, u32[]{:S(2)}, u32[]{:S(2)}) async-start(bf16[16,128,1,128]{3,1,2,0:T(8,128)(2,1)} %bitcast.154), calls=%async_computation.1 | async-start | bytes 1048576 | tf_op jit(solution)/shard_map/all_to_all | solution.py:66
  32.3 1.2 copy-start.2
  111.5 60.6 %all-to-all-start.3 = ((f32[32,4,16,1,128]{4,2,1,3,0:T(8,128)}), f32[32,4,16,1,128]{4,2,1,3,0:T(8,128)}, u32[]{:S(2)}, u32[]{:S(2)}) async-start(f32[32,4,16,1,128]{4,2,1,3,0:T(8,128)} %bitcast.151), calls=%async_computation.3 | async-start | bytes 2097152 | tf_op jit(solution)/shard_map/all_to_all | solution.py:78
  172.2 2.9 %copy-start.1 = (f32[32,4,16,128]{3,0,2,1:T(8,128)S(1)}, f32[32,4,16,128]{3,0,2,1:T(8,128)}, u32[]{:S(2)}) copy-start(f32[32,4,16,128]{3,0,2,1:T(8,128)} %fusion.8) | copy-start | bytes 3145732
  193.6 5.6 %copy-start.4 = (bf16[4,128,128]{2,1,0:T(8,128)(2,1)S(1)}, bf16[4,128,128]{2,1,0:T(8,128)(2,1)}, u32[]{:S(2)}) copy-start(bf16[4,128,128]{2,1,0:T(8,128)(2,1)} %param.4) | copy-start | bytes 393220
  194.6 38.1 %all-to-all-start.4 = ((bf16[1,4,1,16,32,128]{5,3,1,2,0,4:T(8,128)(2,1)}), bf16[1,4,1,16,32,128]{5,3,1,2,0,4:T(8,128)(2,1)S(1)}, u32[]{:S(2)}, u32[]{:S(2)}) async-start(bf16[1,4,1,16,32,128]{5,3,1,2,0,4:T(8,128)(2,1)} %copy.36), calls=%async_computation.4 | async-start | bytes 1048576 | tf_op jit(solution)/shard_map/all_to_all | solution.py:92
where the time goes:
time: 250 us; the launch traced here: 249 us
  waiting for transfers between devices  101 us (40%)
  blocking collectives  88.6 us (35%)
  matrix products  25.1 us (10%)
  starting transfers between devices  20.5 us (8%)
  local copies, waits for them, and re-layouts  13.1 us (5%)
    all_to_all x1, blocking collectives, per_device(): lax.all_to_all(real_rows.reshape(col_shape), 'col', split_axis=0, concat_...  75.4 us
    all_to_all x1, waiting for transfers between devices, per_device(): lax.all_to_all(imag_rows.reshape(col_shape), 'col', split_axis=0, concat_...  53.1 us
    all_to_all x1, waiting for transfers between devices, per_device(): lax.all_to_all(spectrum, 'col', split_axis=4, concat_axis=0, tiled=True)  33.3 us
    all_to_all x1, blocking collectives, per_device(): lax.all_to_all(grouped, 'row', split_axis=2, concat_axis=0, tiled=True)  13.2 us
    convert_element_type x3, local copies, waits for them, and re-layouts, per_device(): spectrum = (spectrum * norm_factor).astype(jnp.bfloat16)  12.6 us
    all_to_all x1, starting transfers between devices, per_device(): lax.all_to_all(row_send[0].astype(jnp.bfloat16), 'row', split_axis=0, con...  7.57 us
    all_to_all x1, waiting for transfers between devices, per_device(): lax.all_to_all(row_send[1].astype(jnp.bfloat16), 'row', split_axis=0, con...  7.44 us
    all_to_all x1, waiting for transfers between devices, per_device(): lax.all_to_all(row_send[0].astype(jnp.bfloat16), 'row', split_axis=0, con...  7.38 us
  transfers between devices with their start and end apart: 4, of which 4 were waited for; matrix products, arithmetic and copies ran while one was open for 3% of the time, Pallas kernels for 0%

commit v1 on v0

v1 whole, which is shorter than its diff:
```python
import functools
import math

import jax
import jax.numpy as jnp
import numpy as np
from jax import lax
from jax.experimental import pallas as pl
from jax.experimental.pallas import tpu as pltpu
from jax.sharding import PartitionSpec as P

MESH = pl.DeviceIdType.MESH
F32, BF16 = jnp.float32, jnp.bfloat16
LENGTH, WIDTH = 65536, 128


def lane_roll(x, shift):
    return pltpu.roll(x, shift % 128, 1)


def lanes(shape):
    return lax.broadcasted_iota(jnp.int32, shape, len(shape) - 1)


def real_fft(xs):
    n = len(xs)
    if n == 1:
        return [xs[0]], [None]
    m = n // 2
    pe, qe = real_fft(xs[0::2])
    po, qo = real_fft(xs[1::2])
    ps, qs = [None] * (m + 1), [None] * (m + 1)
    ps[0], ps[m] = pe[0] + po[0], pe[0] - po[0]
    for k in range(1, m // 2 + (m % 2)):
        c, s = math.cos(2 * math.pi * k / n), math.sin(2 * math.pi * k / n)
        tr = c * po[k] + s * qo[k]
        ti = c * qo[k] - s * po[k]
        ps[k], qs[k] = pe[k] + tr, qe[k] + ti
        ps[m - k], qs[m - k] = pe[k] - tr, ti - qe[k]
    if m % 2 == 0:
        ps[m // 2], qs[m // 2] = pe[m // 2], -po[m // 2]
    return ps, qs


def row_stage(blocks, cos1, sin1, h, roll):
    lane = lanes(blocks[0].shape)
    sgn = jnp.where(lane < 64, -1.0, 1.0).astype(F32)
    special = jnp.logical_and(lane % 32 == 0, h == 0)
    sp_re = jnp.logical_and(special, lane < 64)
    sp_im = jnp.logical_and(special, lane >= 64)
    ps, qs = real_fft(blocks)
    ys = [None] * 16
    ys[0], ys[8] = ps[0], ps[8]
    for d in range(1, 8):
        rolled = roll(qs[d], 64)
        turned = sgn * rolled
        ys[d] = jnp.where(sp_re, ps[d], jnp.where(sp_im, rolled, ps[d] + turned))
        ys[16 - d] = jnp.where(sp_re, roll(ps[d], 64), jnp.where(sp_im, -qs[d], ps[d] - turned))
    outs = [ys[0]]
    cc, ss = cos1, sin1
    for d in range(1, 16):
        outs.append(ys[d] * cc + roll(ys[d], 64) * ss)
        if d < 15:
            cc, ss = cc * cos1 - ss * sin1, ss * cos1 + cc * sin1
    return outs


def block_transpose(tiles, lane, roll):
    a0, a1, a2, a3 = tiles
    low = lane < 64
    b0, b2 = jnp.where(low, a0, roll(a2, 64)), jnp.where(low, roll(a0, 64), a2)
    b1, b3 = jnp.where(low, a1, roll(a3, 64)), jnp.where(low, roll(a1, 64), a3)
    even = (lane // 32) % 2 == 0
    return (
        jnp.where(even, b0, roll(b1, 32)),
        jnp.where(even, roll(b0, 96), b1),
        jnp.where(even, b2, roll(b3, 32)),
        jnp.where(even, roll(b2, 96), b3),
    )


def col_stage(blocks, cos1, sin1, z, h, roll):
    lane = lanes(blocks[0].shape)
    sgn = jnp.where(lane < 64, -1.0, 1.0).astype(F32)
    kappa = -sgn
    device = jnp.logical_and(h == 0, lax.rem(z, 8) == 0)
    special = jnp.logical_and(lane % 32 == 0, device)
    zero_mask = jnp.logical_and(lane >= 0, z == 0)
    ps, qs = real_fft(blocks)
    ws = [None] * 32
    ws[0], ws[16] = ps[0], ps[16]
    for e in range(1, 16):
        turned = sgn * roll(qs[e], 64)
        ws[e], ws[32 - e] = ps[e] + turned, ps[e] - turned
    rolled = [roll(w, 64) for w in ws]
    cc, ss = cos1, sin1
    plus, hs = [ws[0]], [kappa * ws[0]]
    for e in range(1, 33):
        v = (32 - e) % 32
        hs.append(kappa * (ws[v] * cc - rolled[v] * ss))
        if e < 32:
            plus.append(ws[e] * cc + rolled[e] * ss)
            cc, ss = cc * cos1 - ss * sin1, ss * cos1 + cc * sin1
    tiles = [[], []]
    for e in range(32):
        gp, gm = plus[e], jnp.where(zero_mask, hs[e], hs[e + 1])
        half = 0.5 * (gp - gm)
        tiles[0].append(jnp.where(special, gp - half, gp))
        tiles[1].append(jnp.where(special, kappa * roll(half, 64), gm))
    return [
        [block_transpose(tiles[sign][4 * group : 4 * group + 4], lane, roll) for group in range(8)]
        for sign in range(2)
    ]


@functools.cache
def tables():
    ch = np.arange(128)
    maps = np.zeros((2, 128, 2, 2, 2, 32))
    for h in range(2):
        for li in range(32):
            l = 32 * h + li
            re = np.cos(2 * np.pi * ((ch * l) % 128) / 128)
            im = -np.sin(2 * np.pi * ((ch * l) % 128) / 128) if l else np.cos(np.pi * ch)
            for ph in range(2):
                maps[ph, :, h, 0, ph, li] = re
                maps[ph, :, h, 1, ph, li] = im
    maps = maps.reshape(256, 256)
    lane = np.arange(128)
    ph = (lane // 32) % 2
    kap = np.where(lane < 64, 1.0, -1.0)
    pos = 64 * ph[None, :] + np.arange(64)[:, None]
    row_pos = np.stack([pos, pos + 128])
    row_tab = np.stack([np.cos(2 * np.pi * row_pos / LENGTH), kap * np.sin(2 * np.pi * row_pos / LENGTH)])
    zs = 2 * np.pi * np.arange(16) * 256 / LENGTH
    z_tab = np.stack([np.cos(zs), np.sin(zs)])
    col_tab = np.stack([np.cos(2 * np.pi * pos / 4096), kap * np.sin(2 * np.pi * pos / 4096)])
    f = (8 * np.arange(16)[None, :] + np.arange(8)[:, None]).reshape(128)
    full = np.arange(128)
    ang = 2 * np.pi * ((f[:, None] * full[None, :]) % 128) / 128
    last = np.concatenate([np.cos(ang), np.sin(ang)], axis=1) / math.sqrt(LENGTH * WIDTH)
    flip = np.zeros((2, 16, 16, 16, 16))
    for fh in range(16):
        for d in range(16):
            flip[0, fh, d, d, fh] = 1
            flip[1, fh, d, (16 - d) % 16, fh] = 1
    flip = flip.reshape(2, 256, 256)
    pick = np.zeros((128, 128))
    for l in range(64):
        pick[l, l] = 1
        pick[64 + l, 128 - l if l else 64] = 1
    return {
        "maps": maps.astype(BF16),
        "row": row_tab.astype(np.float32),
        "z": z_tab.astype(np.float32),
        "col": col_tab.astype(np.float32),
        "last": last.astype(BF16),
        "flip": flip.astype(BF16),
        "pick": pick.astype(BF16),
    }


def mix_kernel(
    x_ref, maps_ref, row_ref, z_ref, col_ref, last_ref, flip_ref, out_ref,
    t_buf, r_buf, v_buf, w_buf, k_buf, o_buf, i_buf, j_buf, l_buf, send_sem, recv_sem,
):
    row = lax.axis_index("row")
    col = lax.axis_index("col")
    z = col // 2
    h = col % 2
    me = 2 * row + h

    def rc_peer(step):
        peer = lax.rem(me + step, 32)
        return peer, (peer // 2, 2 * z + peer % 2)

    def z_peer(step):
        peer = lax.rem(z + step, 16)
        return peer, (row, 2 * peer + h)

    barrier = pltpu.get_barrier_semaphore()

    def greet_rc(step, carry):
        pl.semaphore_signal(barrier, inc=1, device_id=rc_peer(step)[1], device_id_type=MESH)
        return carry

    def greet_z(step, carry):
        pl.semaphore_signal(barrier, inc=1, device_id=z_peer(step)[1], device_id_type=MESH)
        return carry

    lax.fori_loop(1, 16, greet_z, 0)
    lax.fori_loop(1, 32, greet_rc, 0)

    for s in range(4):
        lhs = jnp.concatenate(
            [
                jnp.concatenate(
                    [x_ref[s, 0:64, 128 * g : 128 * g + 128], x_ref[s, 64:128, 128 * g : 128 * g + 128]], axis=1
                )
                for g in range(4)
            ],
            axis=0,
        )
        res = jnp.dot(lhs, maps_ref[...], preferred_element_type=F32).astype(BF16)
        for g in range(4):
            for half in range(2):
                t_buf[2 * (4 * s + g) + half] = res[64 * g : 64 * g + 64, 128 * half : 128 * half + 128]

    pl.semaphore_wait(barrier, 46)

    def exchange(phase, src, dst, count, peer_of, slot, order):
        def start(step, carry):
            peer, device = peer_of(step)
            pltpu.make_async_remote_copy(
                src_ref=src.at[peer], dst_ref=dst.at[slot], send_sem=send_sem.at[phase], recv_sem=recv_sem.at[phase],
                device_id=device, device_id_type=MESH,
            ).start()
            return carry

        if order is None:
            lax.fori_loop(1, count, start, 0)
        else:
            for step in order:
                start(step, 0)
        dst[slot] = src[slot]

    def finish(phase, src, dst, count):
        pltpu.make_async_copy(src.at[pl.ds(0, count - 1)], dst.at[pl.ds(0, count - 1)], recv_sem.at[phase]).wait()

    def drain(phase, src, dst, count):
        pltpu.make_async_copy(src.at[pl.ds(0, count - 1)], dst.at[pl.ds(0, count - 1)], send_sem.at[phase]).wait()

    far_first = [8, 7, 9, 6, 10, 5, 11, 4, 12, 3, 13, 2, 14, 1, 15]
    exchange(0, t_buf, r_buf, 32, rc_peer, me, None)
    finish(0, t_buf, r_buf, 32)

    zc, zs = z_ref[0, z], z_ref[1, z]

    def row_body(step, carry):
        pc, rows = step // 4, pl.ds(pl.multiple_of(16 * (step % 4), 16), 16)
        kap = jnp.where(lanes((16, 128)) < 64, 1.0, -1.0).astype(F32)
        base_c, base_s = row_ref[0, pc, rows, :], row_ref[1, pc, rows, :]
        cos1 = base_c * zc - base_s * (kap * zs)
        sin1 = base_s * zc + base_c * (kap * zs)
        blocks = [r_buf[2 * a + pc, rows, :].astype(F32) for a in range(16)]
        outs = row_stage(blocks, cos1, sin1, h, lane_roll)
        for d in range(16):
            v_buf[d, pc, rows, :] = outs[d].astype(BF16)
        return carry

    lax.fori_loop(0, 8, row_body, 0)
    exchange(1, v_buf, w_buf, 16, z_peer, z, far_first)
    finish(1, v_buf, w_buf, 16)

    def col_body(step, carry):
        rows = pl.ds(pl.multiple_of(16 * step, 16), 16)
        blocks = [w_buf[q // 2, q % 2, rows, :].astype(F32) for q in range(32)]
        res = col_stage(blocks, col_ref[0, rows, :], col_ref[1, rows, :], z, h, lane_roll)
        for sign in range(2):
            for group in range(8):
                for part in range(4):
                    k_buf[sign, group, part, rows, :] = res[sign][group][part].astype(BF16)
        return carry

    lax.fori_loop(0, 4, col_body, 0)

    for sign in range(2):
        for pair in range(4):
            rhs = jnp.concatenate([k_buf[sign, 2 * pair + i].reshape(256, 128) for i in range(2)], axis=1)
            res = jnp.dot(last_ref[...], rhs, preferred_element_type=F32).astype(BF16)
            for fl in range(8):
                for i in range(2):
                    o_buf[2 * fl + pair // 2, sign, pair % 2, i] = res[16 * fl : 16 * fl + 16, 128 * i : 128 * i + 128]

    exchange(2, o_buf, i_buf, 16, z_peer, z, far_first)
    finish(2, o_buf, i_buf, 16)

    for sign in range(2):
        rhs = jnp.concatenate([i_buf[:, sign, e3, e2].reshape(256, 128) for e3 in range(2) for e2 in range(2)], axis=1)
        res = jnp.dot(flip_ref[sign], rhs, preferred_element_type=F32).astype(BF16)
        for fh in range(16):
            for e3 in range(2):
                for e2 in range(2):
                    at = 128 * (2 * e3 + e2)
                    j_buf[2 * fh + e3, sign, e2] = res[16 * fh : 16 * fh + 16, at : at + 128]

    exchange(3, j_buf, l_buf, 32, rc_peer, me, None)
    finish(3, j_buf, l_buf, 32)
    out_ref[...] = l_buf[...]
    drain(0, t_buf, r_buf, 32)
    drain(1, v_buf, w_buf, 16)
    drain(2, o_buf, i_buf, 16)
    drain(3, j_buf, l_buf, 32)


def spectrum_rows(tiles, roll):
    lane = lanes(tiles[0].shape)
    d = lax.broadcasted_iota(jnp.int32, tiles[0].shape, 0)
    swap = jnp.logical_and(d >= 9, lane % 32 == 0)
    first, third = jnp.where(swap, tiles[2], tiles[0]), jnp.where(swap, tiles[0], tiles[2])
    return block_transpose((first, tiles[1], third, tiles[3]), lane, roll)


def out_kernel(l_ref, group_ref, pick_ref, map_ref, out_ref, spec_buf, chosen_buf):
    @pl.when(pl.program_id(0) == 0)
    def _():
        for g in range(4):
            chosen_buf[g] = jnp.dot(pick_ref[...], group_ref[g], preferred_element_type=F32).astype(BF16)

    grouped = []
    for g in range(4):
        for e2 in range(2):
            tiles = [l_ref[2 * g + hh, sign, e2].astype(F32) for sign in range(2) for hh in range(2)]
            for ein, tile in enumerate(spectrum_rows(tiles, lane_roll)):
                at = 16 * (4 * e2 + ein)
                spec_buf[g, at : at + 16, :] = tile.astype(BF16)
        grouped.append(jnp.dot(spec_buf[g], chosen_buf[g], preferred_element_type=F32).astype(BF16))
    out_ref[0] = jnp.dot(jnp.concatenate(grouped, axis=1), map_ref[...], preferred_element_type=F32).astype(BF16)


def per_device(mix_input, group_maps, out_map):
    tab = tables()
    vmem = pl.BlockSpec(memory_space=pltpu.VMEM)
    landed = pl.pallas_call(
        mix_kernel,
        out_shape=jax.ShapeDtypeStruct((32, 2, 2, 16, 128), BF16),
        in_specs=[vmem, vmem, vmem, pl.BlockSpec(memory_space=pltpu.SMEM), vmem, vmem, vmem],
        out_specs=vmem,
        scratch_shapes=[
            pltpu.VMEM((32, 64, 128), BF16),
            pltpu.VMEM((32, 64, 128), BF16),
            pltpu.VMEM((16, 2, 64, 128), BF16),
            pltpu.VMEM((16, 2, 64, 128), BF16),
            pltpu.VMEM((2, 8, 4, 64, 128), BF16),
            pltpu.VMEM((16, 2, 2, 2, 16, 128), BF16),
            pltpu.VMEM((16, 2, 2, 2, 16, 128), BF16),
            pltpu.VMEM((32, 2, 2, 16, 128), BF16),
            pltpu.VMEM((32, 2, 2, 16, 128), BF16),
            pltpu.SemaphoreType.DMA((4,)),
            pltpu.SemaphoreType.DMA((4,)),
        ],
        compiler_params=pltpu.CompilerParams(collective_id=0, has_side_effects=True, vmem_limit_bytes=32 * 2**20),
    )(mix_input, *(jnp.asarray(tab[name]) for name in ("maps", "row", "z", "col", "last", "flip")))
    return pl.pallas_call(
        out_kernel,
        grid=(4,),
        out_shape=jax.ShapeDtypeStruct((4, 128, out_map.shape[1]), BF16),
        in_specs=[
            pl.BlockSpec((8, 2, 2, 16, 128), lambda s: (s, 0, 0, 0, 0)),
            pl.BlockSpec((4, 128, 128), lambda s: (0, 0, 0)),
            pl.BlockSpec((128, 128), lambda s: (0, 0)),
            pl.BlockSpec(out_map.shape, lambda s: (0, 0)),
        ],
        out_specs=pl.BlockSpec((1, 128, out_map.shape[1]), lambda s: (s, 0, 0)),
        scratch_shapes=[pltpu.VMEM((4, 128, 128), BF16), pltpu.VMEM((4, 128, 128), BF16)],
    )(landed, group_maps, jnp.asarray(tab["pick"]), out_map)


def solution(mesh):
    return jax.shard_map(
        per_device,
        mesh=mesh,
        in_specs=(P(None, ("row", "col"), None), P(), P()),
        out_specs=P(None, ("row", "col"), None),
        check_vma=False,
    )
```

time: 250 us -> 102 us (0.41)
  waiting for transfers between devices: 101 us -> 0 us
  Pallas kernels: 0 us -> 94.7 us
  blocking collectives: 88.6 us -> 0 us
  matrix products: 25.1 us -> 0 us
  starting transfers between devices: 20.5 us -> 0 us
  local copies, waits for them, and re-layouts: 13.1 us -> 6.94 us
    all_to_all x4 -> x0, waiting for transfers between devices: 101 us -> none  [the longest x1 53.1 us: per_device(): lax.all_to_all(imag_rows.reshape(col_shape), 'col', split_axis=0, concat_...]
    pallas_call x0 -> x2, Pallas kernels: none -> 94.7 us  [the longest x1 88.6 us: per_device(): pl.pallas_call(mix_kernel, out_shape=jax.ShapeDtypeStruct((32, 2, 2, 16,...]
    all_to_all x2 -> x0, blocking collectives: 88.6 us -> none  [the longest x1 75.4 us: per_device(): lax.all_to_all(real_rows.reshape(col_shape), 'col', split_axis=0, concat_...]
    dot_general x15 -> x0, matrix products: 25.1 us -> none  [the longest x2 4.29 us: transform(): jnp.einsum(einsum_form, real_in, cosine, precision=precise)]
    all_to_all x4 -> x0, starting transfers between devices: 20.5 us -> none  [the longest x1 7.57 us: per_device(): lax.all_to_all(row_send[0].astype(jnp.bfloat16), 'row', split_axis=0, con...]
    convert_element_type x3 -> x0, local copies, waits for them, and re-layouts: 12.6 us -> none  [per_device(): spectrum = (spectrum * norm_factor).astype(jnp.bfloat16)]
    unnamed x10 -> x16, local copies, waits for them, and re-layouts: 0.51 us -> 6.94 us
  transfers between devices with their start and end apart: 4 -> 0, of which waited for: 4 -> 0; matrix products, arithmetic and copies ran while one was open for 3% -> 0% of each run, Pallas kernels for 0% -> 0%
where the time goes in v1:
time: 102 us
  Pallas kernels  94.7 us (93%)
  local copies, waits for them, and re-layouts  6.94 us (7%)
    pallas_call x1, Pallas kernels, per_device(): pl.pallas_call(mix_kernel, out_shape=jax.ShapeDtypeStruct((32, 2, 2, 16,...  88.6 us
    unnamed x16, local copies, waits for them, and re-layouts  6.94 us
    pallas_call x1, Pallas kernels, per_device(): pl.pallas_call(out_kernel, grid=(4,), out_shape=jax.ShapeDtypeStruct((4,...  6.05 us

profile of v1, /device:TPU:1, one launch (start us, length us, event | category | flops | bytes accessed | tf_op | source)
XLA Modules:
  0.0 101.7 jit_solution(18126229534182862031)
XLA Ops:
  0.0 0.0 copy-start.1
  0.0 1.0 %copy-done.1 = bf16[4,128,512]{2,1,0:T(8,128)(2,1)S(1)} copy-done((bf16[4,128,512]{2,1,0:T(8,128)(2,1)S(1)}, bf16[4,128,512]{2,1,0:T(8,128)(2,1)}, u32[]{:S(2)}) %copy-start.1) | copy-done | bytes 524312
  1.0 0.0 copy-start.2
  1.0 0.9 copy-done.2
  2.0 0.0 copy-start.3
  2.0 0.9 copy-done.3
  2.9 0.0 copy-start.4
  2.9 0.9 copy-done.4
  3.8 0.0 copy-start.5
  3.8 0.8 copy-done.5
  4.6 0.0 copy-start.6
  4.6 0.8 copy-done.6
  5.5 0.0 copy-start.7
  5.5 0.7 copy-done.7
  6.2 88.6 %shard_map.100.l_ref = bf16[32,2,2,16,128]{4,3,2,1,0:T(8,128)(2,1)S(1)} custom-call(bf16[4,128,512]{2,1,0:T(8,128)(2,1)S(1)} %copy-done.1, bf16[256,256]{1,0:T(8,128)(2,1)S(1)} %copy-done.4, f32[2,2,64,128]{3,2,1,0:T(8,128)S(1)} %copy-done.3, f32[2,16]{1,0:T(2,128)S(1)} %copy-done.7, f32[2,64,128]{2,1,0:T(8,128)S(1)} %copy-done.6, ...), custom_call_target="tpu_custom_call" | custom-call | tf_op jit(solution)/shard_map/pallas_call | solution.py:324
  94.8 0.0 copy-start
  94.8 0.8 copy-done
  95.6 6.0 %shard_map.101 = bf16[4,128,2048]{2,1,0:T(8,128)(2,1)} custom-call(bf16[32,2,2,16,128]{4,3,2,1,0:T(8,128)(2,1)} %copy-done, bf16[4,128,128]{2,1,0:T(8,128)(2,1)} %group_ref.1, bf16[128,128]{1,0:T(8,128)(2,1)} %constant.20.clone.pick_ref, bf16[512,2048]{1,0:T(8,128)(2,1)} %map_ref.1), custom_call_target="tpu_custom_call" | custom-call | tf_op jit(solution)/shard_map/pallas_call | solution.py:344
Async XLA Ops:
  0.0 1.0 %copy-start.1 = (bf16[4,128,512]{2,1,0:T(8,128)(2,1)S(1)}, bf16[4,128,512]{2,1,0:T(8,128)(2,1)}, u32[]{:S(2)}) copy-start(bf16[4,128,512]{2,1,0:T(8,128)(2,1)} %x_ref.1) | copy-start | bytes 1572868
  1.0 0.9 copy-start.2
  2.0 0.9 copy-start.3
  2.9 0.9 copy-start.4
  3.8 0.8 copy-start.5
  4.6 0.8 copy-start.6
  5.5 0.7 copy-start.7
  94.8 0.8 copy-start

commit v2 on v1

v2 whole, which is shorter than its diff:
```python
import functools
import math

import jax
import jax.numpy as jnp
import numpy as np
from jax import lax
from jax.experimental import pallas as pl
from jax.experimental.pallas import tpu as pltpu
from jax.sharding import PartitionSpec as P

MESH = pl.DeviceIdType.MESH
F32, BF16 = jnp.float32, jnp.bfloat16
LENGTH, WIDTH = 65536, 128


def lane_roll(x, shift):
    return pltpu.roll(x, shift % 128, 1)


def lanes(shape):
    return lax.broadcasted_iota(jnp.int32, shape, len(shape) - 1)


def real_fft(xs):
    n = len(xs)
    if n == 1:
        return [xs[0]], [None]
    m = n // 2
    pe, qe = real_fft(xs[0::2])
    po, qo = real_fft(xs[1::2])
    ps, qs = [None] * (m + 1), [None] * (m + 1)
    ps[0], ps[m] = pe[0] + po[0], pe[0] - po[0]
    for k in range(1, m // 2 + (m % 2)):
        c, s = math.cos(2 * math.pi * k / n), math.sin(2 * math.pi * k / n)
        tr = c * po[k] + s * qo[k]
        ti = c * qo[k] - s * po[k]
        ps[k], qs[k] = pe[k] + tr, qe[k] + ti
        ps[m - k], qs[m - k] = pe[k] - tr, ti - qe[k]
    if m % 2 == 0:
        ps[m // 2], qs[m // 2] = pe[m // 2], -po[m // 2]
    return ps, qs


def row_stage(blocks, cos1, sin1, has_zero, roll):
    lane = lanes(blocks[0].shape)
    sgn = jnp.where(lane < 64, -1.0, 1.0).astype(F32)
    ps, qs = real_fft(blocks)
    ys = [None] * 16
    ys[0], ys[8] = ps[0], ps[8]
    if has_zero is not None:
        special = jnp.logical_and(lane % 16 == 0, has_zero)
        sp_re = jnp.logical_and(special, lane < 64)
        sp_im = jnp.logical_and(special, lane >= 64)
    for d in range(1, 8):
        rolled = roll(qs[d], 64)
        turned = sgn * rolled
        ys[d], ys[16 - d] = ps[d] + turned, ps[d] - turned
        if has_zero is not None:
            ys[d] = jnp.where(sp_re, ps[d], jnp.where(sp_im, rolled, ys[d]))
            ys[16 - d] = jnp.where(sp_re, roll(ps[d], 64), jnp.where(sp_im, -qs[d], ys[16 - d]))
    outs = [ys[0]]
    cc, ss = cos1, sin1
    for d in range(1, 16):
        outs.append(ys[d] * cc + roll(ys[d], 64) * ss)
        if d < 15:
            cc, ss = cc * cos1 - ss * sin1, ss * cos1 + cc * sin1
    return outs


def block_transpose(tiles, roll):
    tiles = list(tiles)
    block = lanes(tiles[0].shape) // 16
    for dist in (4, 2, 1):
        keep = (block // dist) % 2 == 0
        for i in range(8):
            if i & dist == 0:
                a, b = tiles[i], tiles[i + dist]
                tiles[i] = jnp.where(keep, a, roll(b, 16 * dist))
                tiles[i + dist] = jnp.where(keep, roll(a, 128 - 16 * dist), b)
    return tiles


def col_stage(blocks, cos1, sin1, z, has_zero, roll):
    lane = lanes(blocks[0].shape)
    sgn = jnp.where(lane < 64, -1.0, 1.0).astype(F32)
    kappa = -sgn
    zero_mask = jnp.logical_and(lane >= 0, z == 0)
    ps, qs = real_fft(blocks)
    ws = [None] * 32
    ws[0], ws[16] = ps[0], ps[16]
    for e in range(1, 16):
        turned = sgn * roll(qs[e], 64)
        ws[e], ws[32 - e] = ps[e] + turned, ps[e] - turned
    rolled = [roll(w, 64) for w in ws]
    cc, ss = cos1, sin1
    plus, hs = [ws[0]], [kappa * ws[0]]
    for e in range(1, 33):
        v = (32 - e) % 32
        hs.append(kappa * (ws[v] * cc - rolled[v] * ss))
        if e < 32:
            plus.append(ws[e] * cc + rolled[e] * ss)
            cc, ss = cc * cos1 - ss * sin1, ss * cos1 + cc * sin1
    tiles = [plus, [jnp.where(zero_mask, hs[e], hs[e + 1]) for e in range(32)]]
    if has_zero is not None:
        special = jnp.logical_and(lane % 16 == 0, jnp.logical_and(has_zero, lax.rem(z, 8) == 0))
        for e in range(32):
            gp, gm = tiles[0][e], tiles[1][e]
            half = 0.5 * (gp - gm)
            tiles[0][e] = jnp.where(special, gp - half, gp)
            tiles[1][e] = jnp.where(special, kappa * roll(half, 64), gm)
    return [[block_transpose(tiles[sign][8 * g : 8 * g + 8], roll) for g in range(4)] for sign in range(2)]


def spectrum_rows(tiles, has_zero, roll):
    tiles = list(tiles)
    if has_zero:
        d = lax.broadcasted_iota(jnp.int32, tiles[0].shape, 0)
        swap = jnp.logical_and(d >= 9, lanes(tiles[0].shape) % 16 == 0)
        for i in (0, 4):
            tiles[i], tiles[i + 2] = jnp.where(swap, tiles[i + 2], tiles[i]), jnp.where(swap, tiles[i], tiles[i + 2])
    return block_transpose(tiles, roll)


@functools.cache
def tables():
    ch = np.arange(128)
    maps = np.zeros((4, 128, 2, 2, 2, 4, 16))
    for c in range(2):
        for h in range(2):
            for li in range(16):
                l = 32 * h + 16 * c + li
                re = np.cos(2 * np.pi * ((ch * l) % 128) / 128)
                im = -np.sin(2 * np.pi * ((ch * l) % 128) / 128) if l else np.cos(np.pi * ch)
                for ph in range(4):
                    maps[ph, :, c, h, 0, ph, li] = re
                    maps[ph, :, c, h, 1, ph, li] = im
    lane = np.arange(128)
    kap = np.where(lane < 64, 1.0, -1.0)
    pos = 32 * ((lane // 16) % 4)[None, :] + np.arange(32)[:, None]
    row_pos = np.stack([pos, pos + 128])[None] + 256 * np.arange(16)[:, None, None, None]
    row_tab = np.stack([np.cos(2 * np.pi * row_pos / LENGTH), kap * np.sin(2 * np.pi * row_pos / LENGTH)], axis=1)
    col_tab = np.stack([np.cos(2 * np.pi * pos / 4096), kap * np.sin(2 * np.pi * pos / 4096)])
    f = (8 * np.arange(16)[None, :] + np.arange(8)[:, None]).reshape(128)
    ang = 2 * np.pi * ((f[:, None] * np.arange(128)[None, :]) % 128) / 128
    last = np.concatenate([np.cos(ang), np.sin(ang)], axis=1) / math.sqrt(LENGTH * WIDTH)
    flip = np.zeros((2, 16, 16, 16, 16))
    for fh in range(16):
        for d in range(16):
            flip[0, fh, d, d, fh] = 1
            flip[1, fh, d, (16 - d) % 16, fh] = 1
    pick = np.zeros((2, 2, 2, 16, 128))
    for c in range(2):
        for h in range(2):
            for li in range(16):
                l = 32 * h + 16 * c + li
                pick[c, 0, h, li, l] = 1
                pick[c, 1, h, li, 128 - l if l else 64] = 1
    return {
        "maps": maps.reshape(512, 512).astype(BF16),
        "row": row_tab.astype(np.float32),
        "col": col_tab.astype(np.float32),
        "last": last.astype(BF16),
        "flip": flip.reshape(2, 256, 256).astype(BF16),
        "pick": pick.reshape(128, 128).astype(BF16),
    }


FAR_FIRST = (8, 7, 9, 6, 10, 5, 11, 4, 12, 3, 13, 2, 14, 1, 15)


def mix_kernel(
    x_hbm, maps_hbm, row_hbm, col_hbm, last_hbm, flip_hbm, pick_hbm, group_hbm, out_map_hbm, out_ref,
    x_ref, maps_ref, row_ref, col_ref, last_ref, flip_ref, pick_ref, group_ref, out_map_ref,
    t_buf, r_buf, v_buf, w_buf, k_buf, o_buf, i_buf, j_buf, l_buf, fused_buf, spec_buf, acc_buf,
    load_sem, send_sem, recv_sem,
):
    row = lax.axis_index("row")
    col = lax.axis_index("col")
    z = col // 2
    h = col % 2
    me = 2 * row + h

    pairs = (
        (x_hbm, x_ref), (maps_hbm, maps_ref), (row_hbm.at[z], row_ref), (col_hbm, col_ref), (last_hbm, last_ref),
        (flip_hbm, flip_ref), (pick_hbm, pick_ref), (group_hbm, group_ref), (out_map_hbm, out_map_ref),
    )
    loads = [pltpu.make_async_copy(src, dst, load_sem.at[i]) for i, (src, dst) in enumerate(pairs)]
    for load in loads:
        load.start()

    def rc_peer(step):
        peer = lax.rem(me + step, 32)
        return peer, (peer // 2, 2 * z + peer % 2)

    def z_peer(step):
        peer = lax.rem(z + step, 16)
        return peer, (row, 2 * peer + h)

    barrier = pltpu.get_barrier_semaphore()

    def greet_rc(step, carry):
        pl.semaphore_signal(barrier, inc=1, device_id=rc_peer(step)[1], device_id_type=MESH)
        return carry

    def greet_z(step, carry):
        pl.semaphore_signal(barrier, inc=1, device_id=z_peer(step)[1], device_id_type=MESH)
        return carry

    lax.fori_loop(1, 16, greet_z, 0)
    lax.fori_loop(1, 32, greet_rc, 0)

    def exchange(phase, c, src, dst, count, peer_of, slot, order):
        def start(step, carry):
            peer, device = peer_of(step)
            pltpu.make_async_remote_copy(
                src_ref=src.at[c, peer], dst_ref=dst.at[c, slot], send_sem=send_sem.at[phase, c],
                recv_sem=recv_sem.at[phase, c], device_id=device, device_id_type=MESH,
            ).start()
            return carry

        if order is None:
            lax.fori_loop(1, count, start, 0)
        else:
            for step in order:
                start(step, 0)
        dst[c, slot] = src[c, slot]

    def wait_all(sem, buf, c, count):
        span = buf.at[c, pl.ds(0, count - 1)]
        pltpu.make_async_copy(span, span, sem).wait()

    def rc_in(c):
        for s in range(4):
            lhs = jnp.concatenate(
                [
                    jnp.concatenate(
                        [x_ref[s, 32 * ph : 32 * ph + 32, 128 * g : 128 * g + 128] for ph in range(4)], axis=1
                    )
                    for g in range(4)
                ],
                axis=0,
            )
            res = jnp.dot(lhs, maps_ref[:, 256 * c : 256 * c + 256], preferred_element_type=F32).astype(BF16)
            for g in range(4):
                for half in range(2):
                    t_buf[c, 2 * (4 * s + g) + half] = res[32 * g : 32 * g + 32, 128 * half : 128 * half + 128]

    def row_transform(c):
        def body(step, carry):
            pc, rows = step // 2, pl.ds(pl.multiple_of(16 * (step % 2), 16), 16)
            cos1, sin1 = row_ref[0, pc, rows, :], row_ref[1, pc, rows, :]
            blocks = [r_buf[c, 2 * a + pc, rows, :].astype(F32) for a in range(16)]
            outs = row_stage(blocks, cos1, sin1, h == 0 if c == 0 else None, lane_roll)
            for d in range(16):
                v_buf[c, d, pc, rows, :] = outs[d].astype(BF16)
            return carry

        lax.fori_loop(0, 4, body, 0)

    def col_transform(c):
        def body(step, carry):
            rows = pl.ds(pl.multiple_of(16 * step, 16), 16)
            blocks = [w_buf[c, q // 2, q % 2, rows, :].astype(F32) for q in range(32)]
            res = col_stage(
                blocks, col_ref[0, rows, :], col_ref[1, rows, :], z, h == 0 if c == 0 else None, lane_roll
            )
            for sign in range(2):
                for group in range(4):
                    for part in range(8):
                        k_buf[sign, group, part, rows, :] = res[sign][group][part].astype(BF16)
            return carry

        lax.fori_loop(0, 2, body, 0)
        for sign in range(2):
            for e4 in range(2):
                rhs = jnp.concatenate([k_buf[sign, 2 * e4 + e3].reshape(256, 128) for e3 in range(2)], axis=1)
                res = jnp.dot(last_ref[...], rhs, preferred_element_type=F32).astype(BF16)
                for fl in range(8):
                    for e3 in range(2):
                        o_buf[c, 2 * fl + e4, sign, e3] = res[16 * fl : 16 * fl + 16, 128 * e3 : 128 * e3 + 128]

    def flip_rows(c):
        for sign in range(2):
            rhs = jnp.concatenate([i_buf[c, :, sign, e3].reshape(256, 128) for e3 in range(2)], axis=1)
            res = jnp.dot(flip_ref[sign], rhs, preferred_element_type=F32).astype(BF16)
            for fh in range(16):
                for e3 in range(2):
                    j_buf[c, 2 * fh + e3, sign] = res[16 * fh : 16 * fh + 16, 128 * e3 : 128 * e3 + 128]

    def fuse_maps():
        for g in range(4):
            chosen = jnp.dot(pick_ref[...], group_ref[g], preferred_element_type=F32).astype(BF16)
            for n in range(4):
                at = pl.ds(512 * n, 512)
                res = jnp.dot(chosen, out_map_ref[128 * g : 128 * g + 128, at], preferred_element_type=F32).astype(BF16)
                for c in range(2):
                    fused_buf[c, 64 * g : 64 * g + 64, at] = res[64 * c : 64 * c + 64]

    def spectrum(c):
        def body(step, carry):
            s, half = step // 2, step % 2
            tiles = [
                l_buf[c, 4 * step + 2 * gg + hh, sign].astype(F32)
                for gg in range(2)
                for sign in range(2)
                for hh in range(2)
            ]
            for el, tile in enumerate(spectrum_rows(tiles, c == 0, lane_roll)):
                rows = pl.ds(pl.multiple_of(128 * s + 16 * el, 16), 16)
                spec_buf[half, rows, :] = tile.astype(BF16)
            return carry

        lax.fori_loop(0, 8, body, 0)

    def output(c):
        lhs = jnp.concatenate([spec_buf[0], spec_buf[1]], axis=1)

        def body(n, carry):
            at = pl.ds(pl.multiple_of(256 * n, 256), 256)
            res = jnp.dot(lhs, fused_buf[c, :, at], preferred_element_type=F32)
            if c == 0:
                acc_buf[:, at] = res
            else:
                total = (acc_buf[:, at] + res).astype(BF16)
                for s in range(4):
                    out_ref[s, :, at] = total[128 * s : 128 * s + 128]
            return carry

        lax.fori_loop(0, 8, body, 0)

    loads[0].wait()
    loads[1].wait()
    with jax.named_scope("rc_in0"):
        rc_in(0)
    with jax.named_scope("barrier"):
        pl.semaphore_wait(barrier, 46)
    exchange(0, 0, t_buf, r_buf, 32, rc_peer, me, None)
    with jax.named_scope("rc_in1"):
        rc_in(1)
    exchange(0, 1, t_buf, r_buf, 32, rc_peer, me, None)
    loads[2].wait()
    for c in range(2):
        with jax.named_scope("wait_rc_in"):
            wait_all(recv_sem.at[0, c], r_buf, c, 32)
        with jax.named_scope("row_transform"):
            row_transform(c)
        exchange(1, c, v_buf, w_buf, 16, z_peer, z, FAR_FIRST)
    for load in loads[3:]:
        load.wait()
    with jax.named_scope("fuse_maps"):
        fuse_maps()
    for c in range(2):
        with jax.named_scope("wait_z_in"):
            wait_all(recv_sem.at[1, c], w_buf, c, 16)
        with jax.named_scope("col_transform"):
            col_transform(c)
        exchange(2, c, o_buf, i_buf, 16, z_peer, z, FAR_FIRST)
    for c in range(2):
        with jax.named_scope("wait_z_out"):
            wait_all(recv_sem.at[2, c], i_buf, c, 16)
        with jax.named_scope("flip"):
            flip_rows(c)
        exchange(3, c, j_buf, l_buf, 32, rc_peer, me, None)
        with jax.named_scope("wait_rc_out"):
            wait_all(recv_sem.at[3, c], l_buf, c, 32)
        with jax.named_scope("spectrum"):
            spectrum(c)
        with jax.named_scope("output"):
            output(c)
    for c in range(2):
        wait_all(send_sem.at[0, c], t_buf, c, 32)
        wait_all(send_sem.at[1, c], v_buf, c, 16)
        wait_all(send_sem.at[2, c], o_buf, c, 16)
        wait_all(send_sem.at[3, c], j_buf, c, 32)


def per_device(mix_input, group_maps, out_map):
    tab = tables()
    arrays = [mix_input] + [jnp.asarray(tab[name]) for name in ("maps", "row", "col", "last", "flip", "pick")]
    arrays += [group_maps, out_map]
    hbm = pl.BlockSpec(memory_space=pltpu.HBM)
    small = [pltpu.VMEM(a.shape[1:] if i == 2 else a.shape, a.dtype) for i, a in enumerate(arrays)]
    return pl.pallas_call(
        mix_kernel,
        out_shape=jax.ShapeDtypeStruct((4, 128, out_map.shape[1]), BF16),
        in_specs=[hbm] * len(arrays),
        out_specs=pl.BlockSpec(memory_space=pltpu.VMEM),
        scratch_shapes=small
        + [
            pltpu.VMEM((2, 32, 32, 128), BF16),
            pltpu.VMEM((2, 32, 32, 128), BF16),
            pltpu.VMEM((2, 16, 2, 32, 128), BF16),
            pltpu.VMEM((2, 16, 2, 32, 128), BF16),
            pltpu.VMEM((2, 4, 8, 32, 128), BF16),
            pltpu.VMEM((2, 16, 2, 2, 16, 128), BF16),
            pltpu.VMEM((2, 16, 2, 2, 16, 128), BF16),
            pltpu.VMEM((2, 32, 2, 16, 128), BF16),
            pltpu.VMEM((2, 32, 2, 16, 128), BF16),
            pltpu.VMEM((2, 256, out_map.shape[1]), BF16),
            pltpu.VMEM((2, 512, 128), BF16),
            pltpu.VMEM((512, out_map.shape[1]), F32),
            pltpu.SemaphoreType.DMA((9,)),
            pltpu.SemaphoreType.DMA((4, 2)),
            pltpu.SemaphoreType.DMA((4, 2)),
        ],
        compiler_params=pltpu.CompilerParams(collective_id=0, has_side_effects=True, vmem_limit_bytes=64937984),
    )(*arrays)


def solution(mesh):
    return jax.shard_map(
        per_device,
        mesh=mesh,
        in_specs=(P(None, ("row", "col"), None), P(), P()),
        out_specs=P(None, ("row", "col"), None),
        check_vma=False,
    )
```

time: 102 us -> 87.3 us (0.86)
  Pallas kernels: 94.7 us -> 84 us
  local copies, waits for them, and re-layouts: 6.94 us -> 3.16 us
    pallas_call x2 -> x1, Pallas kernels: 94.7 us -> 84 us  [per_device(): pl.pallas_call(mix_kernel, out_shape=jax.ShapeDtypeStruct((4, 128, out_ma...]
    unnamed x16 -> x1, local copies, waits for them, and re-layouts: 6.94 us -> 3.16 us
where the time goes in v2:
time: 87.3 us; the launch traced here: 87.1 us
  Pallas kernels  84 us (96%)
  local copies, waits for them, and re-layouts  3.16 us (4%)
    pallas_call x1, Pallas kernels, per_device(): pl.pallas_call(mix_kernel, out_shape=jax.ShapeDtypeStruct((4, 128, out_ma...  84 us
    unnamed x1, local copies, waits for them, and re-layouts  3.16 us

profile of v2, /device:TPU:1, one launch (start us, length us, event | category | flops | bytes accessed | tf_op | source)
XLA Modules:
  0.0 87.1 jit_solution(4459063427033963048)
XLA Ops:
  0.0 84.0 %shard_map.91 = bf16[4,128,2048]{2,1,0:T(8,128)(2,1)} custom-call(bf16[4,128,512]{2,1,0:T(8,128)(2,1)} %x_hbm.1, bf16[512,512]{1,0:T(8,128)(2,1)} %constant.12.clone.maps_hbm, f32[16,2,2,32,128]{4,3,2,1,0:T(8,128)} %constant.13.clone.row_hbm, f32[2,32,128]{2,1,0:T(8,128)} %constant.14.clone.col_hbm, bf16[128,256]{1,0:T(8,128)(2,1)} %constant.15.clone.last_hbm, ...), custom_call_target="tpu_custom_call" | custom-call | tf_op jit(solution)/shard_map/pallas_call | solution.py:384
  84.0 3.2 %copy.11 = bf16[4,128,2048]{2,1,0:T(8,128)(2,1)} copy(bf16[4,128,2048]{2,1,0:T(8,128)(2,1)} %shard_map.91) | data formatting | bytes 4194304

commit v3 on v0

v3 whole, which is shorter than its diff:
```python
import functools
import math

import jax
import jax.numpy as jnp
import numpy as np
from jax import lax
from jax.experimental import pallas as pl
from jax.experimental.pallas import tpu as pltpu
from jax.sharding import PartitionSpec as P

MESH = pl.DeviceIdType.MESH
F32, BF16 = jnp.float32, jnp.bfloat16
LENGTH, WIDTH = 65536, 128
FAR_FIRST = (8, 7, 9, 6, 10, 5, 11, 4, 12, 3, 13, 2, 14, 1, 15)


@functools.cache
def tables():
    ch = np.arange(128)
    chan = np.zeros((2, 2, 32, 128))
    pick = np.zeros((2, 2, 32, 128))
    for c in range(2):
        for lg in range(32):
            l = 32 * c + lg
            chan[c, 0, lg] = np.cos(2 * np.pi * ((ch * l) % 128) / 128)
            chan[c, 1, lg] = -np.sin(2 * np.pi * ((ch * l) % 128) / 128) if l else np.cos(np.pi * ch)
            if l:
                pick[c, 0, lg, [l, 128 - l]] = 1, 1
                pick[c, 1, lg, [l, 128 - l]] = -1, 1
            else:
                pick[c, 0, lg, 0] = pick[c, 1, lg, 64] = 1
    in_flip = np.zeros((16, 16, 16, 16))
    out_flip = np.zeros((8, 32, 32, 8))
    for i in range(16):
        for j in range(16):
            in_flip[i, j, j, i] = 1
    for i in range(8):
        for j in range(32):
            out_flip[i, j, j, i] = 1
    src = np.arange(512)
    q = 32 * (src // 32) + src // 16 % 2 + 2 * (src % 16)
    k1 = np.arange(512)
    ang = 2 * np.pi * ((k1[:, None] * q[None, :]) % 512) / 512
    turn = 2 * np.pi * k1[:, None] * np.arange(128)[None, :] / LENGTH
    fang = 2 * np.pi * ((np.arange(128)[:, None] * np.arange(128)[None, :]) % 128) / 128
    last = np.stack(
        [np.concatenate([np.cos(fang), np.sin(fang)], axis=1), np.concatenate([-np.sin(fang), np.cos(fang)], axis=1)]
    ) / math.sqrt(LENGTH * WIDTH)
    return {
        "chan": chan.reshape(128, 128).astype(BF16),
        "in_flip": in_flip.reshape(256, 256).astype(BF16),
        "dft": np.concatenate([np.cos(ang), -np.sin(ang)]).astype(BF16),
        "turn": np.stack([np.cos(turn), np.sin(turn)]).astype(np.float32),
        "last": last.astype(BF16),
        "out_flip": out_flip.reshape(256, 256).astype(BF16),
        "pick": pick.reshape(128, 128).astype(BF16),
    }


def mix_kernel(
    x_hbm, chan_hbm, in_flip_hbm, dft_hbm, turn_hbm, last_hbm, out_flip_hbm, pick_hbm, group_hbm, out_ref,
    x_ref, chan_ref, in_flip_ref, dft_ref, turn_ref, last_ref, out_flip_ref, pick_ref, group_ref,
    t_buf, w_buf, v_buf, r_buf, f_buf, g_buf, o_buf, m_buf, j_buf, s_buf, chosen_buf, load_sem, send_sem, recv_sem,
):
    row = lax.axis_index("row")
    col = lax.axis_index("col")
    z = col // 2
    h = col % 2
    me = 2 * row + h

    pairs = tuple((x_hbm.at[s], x_ref.at[s]) for s in range(4)) + (
        (chan_hbm, chan_ref), (in_flip_hbm, in_flip_ref), (dft_hbm, dft_ref), (turn_hbm, turn_ref),
        (last_hbm, last_ref), (out_flip_hbm, out_flip_ref), (pick_hbm, pick_ref), (group_hbm, group_ref),
    )
    loads = [pltpu.make_async_copy(src, dst, load_sem.at[i]) for i, (src, dst) in enumerate(pairs)]
    for load in loads[:5]:
        load.start()

    def rc_peer(step):
        peer = lax.rem(me + step, 32)
        return peer, (peer // 2, 2 * z + peer % 2)

    def z_peer(step):
        peer = lax.rem(z + step, 16)
        return peer, (row, 2 * peer + h)

    barrier = pltpu.get_barrier_semaphore()

    for step in range(1, 16):
        pl.semaphore_signal(barrier, inc=1, device_id=z_peer(step)[1], device_id_type=MESH)
    for step in range(1, 32):
        pl.semaphore_signal(barrier, inc=1, device_id=rc_peer(step)[1], device_id_type=MESH)

    def exchange(phase, c, src, dst, peer_of, slot, order):
        for step in order:
            peer, device = peer_of(step)
            pltpu.make_async_remote_copy(
                src_ref=src.at[c, peer], dst_ref=dst.at[c, slot], send_sem=send_sem.at[phase, c],
                recv_sem=recv_sem.at[phase, c], device_id=device, device_id_type=MESH,
            ).start()
        dst[c, slot] = src[c, slot]

    def wait_all(sem, buf, c, count):
        span = buf.at[c, pl.ds(0, count - 1)]
        pltpu.make_async_copy(span, span, sem).wait()

    def channel_transform():
        for g in range(4):
            rhs = jnp.concatenate([x_ref[s, :, 128 * g : 128 * g + 128] for s in range(4)], axis=0)
            res = lax.dot_general(chan_ref[...], rhs, (((1,), (1,)), ((), ())), preferred_element_type=F32)
            res = res.astype(BF16)
            for c in range(4):
                for s in range(4):
                    t_buf[c, 4 * s + g] = res[32 * c : 32 * c + 32, 128 * s : 128 * s + 128]

    def in_turn(c):
        rhs = jnp.concatenate([w_buf[c, :, 16 * b : 16 * b + 16, :].reshape(256, 128) for b in range(2)], axis=1)
        res = jnp.dot(in_flip_ref[...], rhs, preferred_element_type=F32).astype(BF16)
        for b in range(2):
            for i in range(16):
                v_buf[c, 16 * b + i] = res[16 * i : 16 * i + 16, 128 * b : 128 * b + 128]

    def transform(c):
        f_buf[...] = jnp.dot(dft_ref[...], r_buf[c].reshape(512, 128), preferred_element_type=F32)

        def body(step, carry):
            rows = pl.ds(pl.multiple_of(64 * step, 64), 64)
            under = pl.ds(pl.multiple_of(512 + 64 * step, 64), 64)
            re, im, cos, sin = f_buf[rows, :], f_buf[under, :], turn_ref[0, rows, :], turn_ref[1, rows, :]
            g_buf[rows, 0:128] = (re * cos + im * sin).astype(BF16)
            g_buf[rows, 128:256] = (im * cos - re * sin).astype(BF16)
            return carry

        lax.fori_loop(0, 8, body, 0)
        kind = jnp.where(me == 0, 0, 1) if c == 1 else c % 2
        res = lax.dot_general(
            last_ref[kind], g_buf[...], (((1,), (1,)), ((), ())), preferred_element_type=F32
        ).astype(BF16)
        for fh in range(16):
            for e3 in range(2):
                for e4 in range(2):
                    at = 256 * e4 + 128 * e3
                    o_buf[c, 2 * fh + e3, e4] = res[8 * fh : 8 * fh + 8, at : at + 128]

    def out_turn(c):
        rhs = jnp.concatenate([m_buf[c, :, e4].reshape(256, 128) for e4 in range(2)], axis=1)
        res = jnp.dot(out_flip_ref[...], rhs, preferred_element_type=F32).astype(BF16)
        for fl in range(8):
            for e4 in range(2):
                j_buf[c, 2 * fl + e4] = res[32 * fl : 32 * fl + 32, 128 * e4 : 128 * e4 + 128]

    def choose():
        for g in range(4):
            chosen_buf[g] = jnp.dot(pick_ref[...], group_ref[g], preferred_element_type=F32).astype(BF16)

    def group():
        for g in range(4):
            lhs = jnp.concatenate(
                [
                    jnp.concatenate([s_buf[c, 4 * s + g] for c in range(4)], axis=0)
                    for s in range(4)
                ],
                axis=1,
            )
            res = lax.dot_general(lhs, chosen_buf[g], (((0,), (0,)), ((), ())), preferred_element_type=F32)
            out_ref[:, 128 * g : 128 * g + 128] = res.astype(BF16)

    def scope(name, run, *args):
        with jax.named_scope(name):
            run(*args)

    for load in loads[:5]:
        load.wait()
    scope("channel", channel_transform)
    with jax.named_scope("barrier"):
        pl.semaphore_wait(barrier, 46)
    for c in range(4):
        exchange(0, c, t_buf, w_buf, z_peer, z, FAR_FIRST)
    for load in loads[5:]:
        load.start()
    for load in loads[5:]:
        load.wait()
    scope("choose", choose)

    def z_in(c):
        scope(f"wait_z_in{c}", wait_all, recv_sem.at[0, c], w_buf, c, 16)
        scope(f"in_turn{c}", in_turn, c)
        exchange(1, c, v_buf, r_buf, rc_peer, me, range(1, 32))

    def rc_in(c):
        scope(f"wait_rc_in{c}", wait_all, recv_sem.at[1, c], r_buf, c, 32)
        scope(f"transform{c}", transform, c)
        exchange(2, c, o_buf, m_buf, rc_peer, me, range(1, 32))

    def rc_out(c):
        scope(f"wait_rc_out{c}", wait_all, recv_sem.at[2, c], m_buf, c, 32)
        scope(f"out_turn{c}", out_turn, c)
        exchange(3, c, j_buf, s_buf, z_peer, z, FAR_FIRST)

    order = (
        (z_in, 0), (z_in, 1), (rc_in, 0), (z_in, 2), (rc_in, 1), (rc_out, 0), (z_in, 3), (rc_in, 2), (rc_out, 1),
        (rc_in, 3), (rc_out, 2), (rc_out, 3),
    )
    for stage, c in order:
        stage(c)
    for c in range(4):
        wait_all(send_sem.at[0, c], t_buf, c, 16)
        wait_all(send_sem.at[1, c], v_buf, c, 32)
        wait_all(send_sem.at[2, c], o_buf, c, 32)
    for c in range(4):
        scope(f"wait_z_out{c}", wait_all, recv_sem.at[3, c], s_buf, c, 16)
    scope("group", group)
    for c in range(4):
        wait_all(send_sem.at[3, c], j_buf, c, 16)


def per_device(mix_input, group_maps, out_map):
    tab = tables()
    names = ("chan", "in_flip", "dft", "turn", "last", "out_flip", "pick")
    arrays = [mix_input] + [jnp.asarray(tab[name]) for name in names] + [group_maps]
    hbm = pl.BlockSpec(memory_space=pltpu.HBM)
    grouped = pl.pallas_call(
        mix_kernel,
        out_shape=jax.ShapeDtypeStruct((512, 512), BF16),
        in_specs=[hbm] * len(arrays),
        out_specs=pl.BlockSpec(memory_space=pltpu.VMEM),
        scratch_shapes=[pltpu.VMEM(a.shape, a.dtype) for a in arrays]
        + [
            pltpu.VMEM((4, 16, 32, 128), BF16),
            pltpu.VMEM((4, 16, 32, 128), BF16),
            pltpu.VMEM((4, 32, 16, 128), BF16),
            pltpu.VMEM((4, 32, 16, 128), BF16),
            pltpu.VMEM((1024, 128), F32),
            pltpu.VMEM((512, 256), BF16),
            pltpu.VMEM((4, 32, 2, 8, 128), BF16),
            pltpu.VMEM((4, 32, 2, 8, 128), BF16),
            pltpu.VMEM((4, 16, 32, 128), BF16),
            pltpu.VMEM((4, 16, 32, 128), BF16),
            pltpu.VMEM((4, 128, 128), BF16),
            pltpu.SemaphoreType.DMA((12,)),
            pltpu.SemaphoreType.DMA((4, 4)),
            pltpu.SemaphoreType.DMA((4, 4)),
        ],
        compiler_params=pltpu.CompilerParams(collective_id=0, has_side_effects=True, vmem_limit_bytes=64937984),
    )(*arrays)
    mixed = jnp.dot(grouped, out_map, preferred_element_type=F32).astype(BF16)
    return mixed.reshape(4, 128, out_map.shape[1])


def solution(mesh):
    return jax.shard_map(
        per_device,
        mesh=mesh,
        in_specs=(P(None, ("row", "col"), None), P(), P()),
        out_specs=P(None, ("row", "col"), None),
        check_vma=False,
    )
```

time: 250 us -> 71.8 us (0.29)
  waiting for transfers between devices: 101 us -> 0 us
  blocking collectives: 88.6 us -> 0 us
  Pallas kernels: 0 us -> 67.9 us
  matrix products: 25.1 us -> 3.62 us
  starting transfers between devices: 20.5 us -> 0 us
  local copies, waits for them, and re-layouts: 13.1 us -> 0.01 us
    all_to_all x4 -> x0, waiting for transfers between devices: 101 us -> none  [the longest x1 53.1 us: per_device(): lax.all_to_all(imag_rows.reshape(col_shape), 'col', split_axis=0, concat_...]
    all_to_all x2 -> x0, blocking collectives: 88.6 us -> none  [the longest x1 75.4 us: per_device(): lax.all_to_all(real_rows.reshape(col_shape), 'col', split_axis=0, concat_...]
    pallas_call x0 -> x1, Pallas kernels: none -> 67.9 us  [per_device(): pl.pallas_call(mix_kernel, out_shape=jax.ShapeDtypeStruct((512, 512), BF1...]
    dot_general x15 -> x1, matrix products: 25.1 us -> 3.62 us  [per_device(): mixed = jnp.dot(grouped, out_map, preferred_element_type=F32).astype(BF16)]
    all_to_all x4 -> x0, starting transfers between devices: 20.5 us -> none  [the longest x1 7.57 us: per_device(): lax.all_to_all(row_send[0].astype(jnp.bfloat16), 'row', split_axis=0, con...]
    convert_element_type x3 -> x0, local copies, waits for them, and re-layouts: 12.6 us -> none  [per_device(): spectrum = (spectrum * norm_factor).astype(jnp.bfloat16)]
  transfers between devices with their start and end apart: 4 -> 0, of which waited for: 4 -> 0; matrix products, arithmetic and copies ran while one was open for 3% -> 0% of each run, Pallas kernels for 0% -> 0%
where the time goes in v3:
time: 71.8 us; the launch traced here: 71.6 us
  Pallas kernels  67.9 us (95%)
  matrix products  3.62 us (5%)
    pallas_call x1, Pallas kernels, per_device(): pl.pallas_call(mix_kernel, out_shape=jax.ShapeDtypeStruct((512, 512), BF1...  67.9 us
    dot_general x1, matrix products, per_device(): mixed = jnp.dot(grouped, out_map, preferred_element_type=F32).astype(BF16)  3.62 us

profile of v3, /device:TPU:1, one launch (start us, length us, event | category | flops | bytes accessed | tf_op | source)
XLA Modules:
  0.0 71.6 jit_solution(14178270819449907672)
XLA Ops:
  0.0 0.0 copy-start
  0.0 67.9 %shard_map.100 = bf16[512,512]{1,0:T(8,128)(2,1)} custom-call(bf16[4,128,512]{2,1,0:T(8,128)(2,1)} %x_hbm.1, bf16[128,128]{1,0:T(8,128)(2,1)} %constant.14.clone.chan_hbm, bf16[256,256]{1,0:T(8,128)(2,1)} %constant.15.clone.in_flip_hbm, bf16[1024,512]{1,0:T(8,128)(2,1)} %constant.16.clone.dft_hbm, f32[2,512,128]{2,1,0:T(8,128)} %constant.17.clone.turn_hbm, ...), custom_call_target="tpu_custom_call" | custom-call | tf_op jit(solution)/shard_map/pallas_call | solution.py:223
  67.9 0.0 copy-done
  67.9 3.6 %convolution_convert_fusion = bf16[512,2048]{1,0:T(8,128)(2,1)} fusion(bf16[512,512]{1,0:T(8,128)(2,1)} %shard_map.100, bf16[512,2048]{1,0:T(8,128)(2,1)S(1)} %copy-done), kind=kOutput, calls=%fused_computation | convolution fusion | flops 1074790400 | bytes 4718592 | tf_op jit(solution)/shard_map/dot_general | solution.py:247
Async XLA Ops:
  0.0 67.9 %copy-start = (bf16[512,2048]{1,0:T(8,128)(2,1)S(1)}, bf16[512,2048]{1,0:T(8,128)(2,1)}, u32[]{:S(2)}) copy-start(bf16[512,2048]{1,0:T(8,128)(2,1)} %param.12) | copy-start | bytes 6291460

commit v4 on v3

--- a/solution.py
+++ b/solution.py
@@ -59,9 +59,9 @@
 
 
 def mix_kernel(
-    x_hbm, chan_hbm, in_flip_hbm, dft_hbm, turn_hbm, last_hbm, out_flip_hbm, pick_hbm, group_hbm, out_ref,
-    x_ref, chan_ref, in_flip_ref, dft_ref, turn_ref, last_ref, out_flip_ref, pick_ref, group_ref,
-    t_buf, w_buf, v_buf, r_buf, f_buf, g_buf, o_buf, m_buf, j_buf, s_buf, chosen_buf, load_sem, send_sem, recv_sem,
+    x_hbm, chan_hbm, in_flip_hbm, dft_hbm, turn_hbm, last_hbm, out_flip_hbm, pick_hbm, group_hbm, out_map_hbm,
+    rows_ref, part_ref, late_map_ref, x_ref, chan_ref, in_flip_ref, dft_ref, turn_ref, last_ref, out_flip_ref, pick_ref, group_ref, out_map_ref,
+    t_buf, w_buf, v_buf, r_buf, f_buf, g_buf, o_buf, m_buf, j_buf, s_buf, fused_buf, acc_buf, load_sem, send_sem, recv_sem,
 ):
     row = lax.axis_index("row")
     col = lax.axis_index("col")
@@ -72,6 +72,7 @@
     pairs = tuple((x_hbm.at[s], x_ref.at[s]) for s in range(4)) + (
         (chan_hbm, chan_ref), (in_flip_hbm, in_flip_ref), (dft_hbm, dft_ref), (turn_hbm, turn_ref),
         (last_hbm, last_ref), (out_flip_hbm, out_flip_ref), (pick_hbm, pick_ref), (group_hbm, group_ref),
+        (out_map_hbm, out_map_ref),
     )
     loads = [pltpu.make_async_copy(src, dst, load_sem.at[i]) for i, (src, dst) in enumerate(pairs)]
     for load in loads[:5]:
@@ -150,21 +151,42 @@
             for e4 in range(2):
                 j_buf[c, 2 * fl + e4] = res[32 * fl : 32 * fl + 32, 128 * e4 : 128 * e4 + 128]
 
-    def choose():
+    def fuse_maps():
         for g in range(4):
-            chosen_buf[g] = jnp.dot(pick_ref[...], group_ref[g], preferred_element_type=F32).astype(BF16)
-
-    def group():
-        for g in range(4):
-            lhs = jnp.concatenate(
-                [
-                    jnp.concatenate([s_buf[c, 4 * s + g] for c in range(4)], axis=0)
-                    for s in range(4)
-                ],
-                axis=1,
-            )
-            res = lax.dot_general(lhs, chosen_buf[g], (((0,), (0,)), ((), ())), preferred_element_type=F32)
-            out_ref[:, 128 * g : 128 * g + 128] = res.astype(BF16)
+            chosen = jnp.dot(pick_ref[...], group_ref[g], preferred_element_type=F32).astype(BF16)
+            for n in range(4):
+                at = pl.ds(512 * n, 512)
+                res = jnp.dot(chosen, out_map_ref[128 * g : 128 * g + 128, at], preferred_element_type=F32).astype(BF16)
+                for c in range(3):
+                    fused_buf[c, 32 * g : 32 * g + 32, at] = res[32 * c : 32 * c + 32]
+                late_map_ref[32 * g : 32 * g + 32, at] = res[96:128]
+
+    def spectrum_rows(c):
+        return jnp.concatenate([s_buf[c, 4 * s : 4 * s + 4].reshape(128, 128).T for s in range(4)], axis=0)
+
+    def first_product():
+        lhs = jnp.concatenate([spectrum_rows(0), spectrum_rows(1)], axis=1)
+
+        def body(n, carry):
+            at = pl.ds(pl.multiple_of(256 * n, 256), 256)
+            acc_buf[:, at] = jnp.dot(lhs, fused_buf[0:2, :, at].reshape(256, 256), preferred_element_type=F32)
+            return carry
+
+        lax.fori_loop(0, 8, body, 0)
+
+    def second_product():
+        lhs = spectrum_rows(2)
+
+        def body(n, carry):
+            at = pl.ds(pl.multiple_of(256 * n, 256), 256)
+            res = jnp.dot(lhs, fused_buf[2, :, at], preferred_element_type=F32)
+            part_ref[:, at] = (acc_buf[:, at] + res).astype(BF16)
+            return carry
+
+        lax.fori_loop(0, 8, body, 0)
+
+    def last_rows():
+        rows_ref[...] = spectrum_rows(3)
 
     def scope(name, run, *args):
         with jax.named_scope(name):
@@ -181,7 +203,7 @@
         load.start()
     for load in loads[5:]:
         load.wait()
-    scope("choose", choose)
+    scope("fuse_maps", fuse_maps)
 
     def z_in(c):
         scope(f"wait_z_in{c}", wait_all, recv_sem.at[0, c], w_buf, c, 16)
@@ -204,27 +226,31 @@
     )
     for stage, c in order:
         stage(c)
+    for c in range(2):
+        scope(f"wait_z_out{c}", wait_all, recv_sem.at[3, c], s_buf, c, 16)
+    scope("first_product", first_product)
+    scope("wait_z_out2", wait_all, recv_sem.at[3, 2], s_buf, 2, 16)
+    scope("second_product", second_product)
     for c in range(4):
         wait_all(send_sem.at[0, c], t_buf, c, 16)
         wait_all(send_sem.at[1, c], v_buf, c, 32)
         wait_all(send_sem.at[2, c], o_buf, c, 32)
-    for c in range(4):
-        scope(f"wait_z_out{c}", wait_all, recv_sem.at[3, c], s_buf, c, 16)
-    scope("group", group)
-    for c in range(4):
         wait_all(send_sem.at[3, c], j_buf, c, 16)
+    scope("wait_z_out3", wait_all, recv_sem.at[3, 3], s_buf, 3, 16)
+    scope("last_rows", last_rows)
 
 
 def per_device(mix_input, group_maps, out_map):
     tab = tables()
     names = ("chan", "in_flip", "dft", "turn", "last", "out_flip", "pick")
-    arrays = [mix_input] + [jnp.asarray(tab[name]) for name in names] + [group_maps]
+    arrays = [mix_input] + [jnp.asarray(tab[name]) for name in names] + [group_maps, out_map]
     hbm = pl.BlockSpec(memory_space=pltpu.HBM)
-    grouped = pl.pallas_call(
+    model = out_map.shape[1]
+    rows, part, late_map = pl.pallas_call(
         mix_kernel,
-        out_shape=jax.ShapeDtypeStruct((512, 512), BF16),
+        out_shape=[jax.ShapeDtypeStruct(shape, BF16) for shape in ((512, 128), (512, model), (128, model))],
         in_specs=[hbm] * len(arrays),
-        out_specs=pl.BlockSpec(memory_space=pltpu.VMEM),
+        out_specs=[pl.BlockSpec(memory_space=pltpu.VMEM)] * 3,
         scratch_shapes=[pltpu.VMEM(a.shape, a.dtype) for a in arrays]
         + [
             pltpu.VMEM((4, 16, 32, 128), BF16),
@@ -237,15 +263,16 @@
             pltpu.VMEM((4, 32, 2, 8, 128), BF16),
             pltpu.VMEM((4, 16, 32, 128), BF16),
             pltpu.VMEM((4, 16, 32, 128), BF16),
-            pltpu.VMEM((4, 128, 128), BF16),
-            pltpu.SemaphoreType.DMA((12,)),
+            pltpu.VMEM((3, 128, model), BF16),
+            pltpu.VMEM((512, model), F32),
+            pltpu.SemaphoreType.DMA((13,)),
             pltpu.SemaphoreType.DMA((4, 4)),
             pltpu.SemaphoreType.DMA((4, 4)),
         ],
-        compiler_params=pltpu.CompilerParams(collective_id=0, has_side_effects=True, vmem_limit_bytes=64937984),
-    )(*arrays)
-    mixed = jnp.dot(grouped, out_map, preferred_element_type=F32).astype(BF16)
-    return mixed.reshape(4, 128, out_map.shape[1])
+        compiler_params=pltpu.CompilerParams(collective_id=0, has_side_effects=True, vmem_limit_bytes=40 * 2**20),
+    )(*[pltpu.with_memory_space_constraint(a, pltpu.HBM) for a in arrays])
+    mixed = jnp.dot(rows, late_map, preferred_element_type=F32) + part.astype(F32)
+    return mixed.astype(BF16).reshape(4, 128, model)
 
 
 def solution(mesh):

time: 71.8 us -> 68.9 us (0.960)
  matrix products: 3.62 us -> 2.02 us
  Pallas kernels: 67.9 us -> 66.7 us
    dot_general x1, matrix products: 3.62 us -> 2.02 us  [per_device(): jnp.dot(rows, late_map, preferred_element_type=F32) + part.astype(F32)]
    pallas_call x1, Pallas kernels: 67.9 us -> 66.7 us  [per_device(): pl.pallas_call(mix_kernel, out_shape=[jax.ShapeDtypeStruct(shape, BF16) f...]
where the time goes in v4:
time: 68.9 us; the launch traced here: 68.8 us
  Pallas kernels  66.7 us (97%)
  matrix products  2.02 us (3%)
    pallas_call x1, Pallas kernels, per_device(): pl.pallas_call(mix_kernel, out_shape=[jax.ShapeDtypeStruct(shape, BF16) f...  66.7 us
    dot_general x1, matrix products, per_device(): jnp.dot(rows, late_map, preferred_element_type=F32) + part.astype(F32)  2.02 us

profile of v4, /device:TPU:1, one launch (start us, length us, event | category | flops | bytes accessed | tf_op | source)
XLA Modules:
  0.0 68.8 jit_solution(17059823002992862754)
XLA Ops:
  0.0 66.7 %shard_map.100 = (bf16[512,128]{1,0:T(8,128)(2,1)S(1)}, bf16[512,2048]{1,0:T(8,128)(2,1)S(1)}, bf16[128,2048]{1,0:T(8,128)(2,1)S(1)}) custom-call(bf16[4,128,512]{2,1,0:T(8,128)(2,1)} %x_hbm.1, bf16[128,128]{1,0:T(8,128)(2,1)} %constant.14.clone.chan_hbm, bf16[256,256]{1,0:T(8,128)(2,1)} %constant.15.clone.in_flip_hbm, ...), custom_call_target="tpu_custom_call" | custom-call | tf_op jit(solution)/shard_map/pallas_call | solution.py:249
  66.8 2.0 %add_convert_fusion = bf16[512,2048]{1,0:T(8,128)(2,1)} fusion(bf16[512,2048]{1,0:T(8,128)(2,1)S(1)} %get-tuple-element.10, bf16[512,128]{1,0:T(8,128)(2,1)S(1)} %get-tuple-element.8, bf16[128,2048]{1,0:T(8,128)(2,1)S(1)} %get-tuple-element.9), kind=kOutput, calls=%fused_computation | convolution fusion | flops 271581184 | bytes 4849664 | tf_op jit(solution)/shard_map/dot_general | solution.py:274

commit v5 on v4

--- a/solution.py
+++ b/solution.py
@@ -12,6 +12,14 @@
 MESH = pl.DeviceIdType.MESH
 F32, BF16 = jnp.float32, jnp.bfloat16
 LENGTH, WIDTH = 65536, 128
+SIDE = 4
+HOPS = (0, 1, 2, 1)
+RC_FAR_FIRST = tuple(
+    sorted(
+        ((dy, dx, dh) for dy in range(SIDE) for dx in range(SIDE) for dh in range(2) if dy or dx or dh),
+        key=lambda step: (-HOPS[step[0]] - HOPS[step[1]], step[2], step),
+    )
+)
 FAR_FIRST = (8, 7, 9, 6, 10, 5, 11, 4, 12, 3, 13, 2, 14, 1, 15)
 
 
@@ -75,12 +83,12 @@
         (out_map_hbm, out_map_ref),
     )
     loads = [pltpu.make_async_copy(src, dst, load_sem.at[i]) for i, (src, dst) in enumerate(pairs)]
-    for load in loads[:5]:
-        load.start()
 
     def rc_peer(step):
-        peer = lax.rem(me + step, 32)
-        return peer, (peer // 2, 2 * z + peer % 2)
+        dy, dx, dh = step
+        peer_row = SIDE * lax.rem(row // SIDE + dy, SIDE) + lax.rem(row % SIDE + dx, SIDE)
+        peer_core = lax.rem(h + dh, 2)
+        return 2 * peer_row + peer_core, (peer_row, 2 * z + peer_core)
 
     def z_peer(step):
         peer = lax.rem(z + step, 16)
@@ -88,19 +96,25 @@
 
     barrier = pltpu.get_barrier_semaphore()
 
-    for step in range(1, 16):
+    for step in FAR_FIRST:
         pl.semaphore_signal(barrier, inc=1, device_id=z_peer(step)[1], device_id_type=MESH)
-    for step in range(1, 32):
+    for load in loads[:6]:
+        load.start()
+    for step in RC_FAR_FIRST:
         pl.semaphore_signal(barrier, inc=1, device_id=rc_peer(step)[1], device_id_type=MESH)
 
-    def exchange(phase, c, src, dst, peer_of, slot, order):
+    def exchange(phase, c, src, dst, peer_of, slot, order, part=None):
         for step in order:
             peer, device = peer_of(step)
+            send, land = src.at[c, peer], dst.at[c, slot]
+            if part is not None:
+                send, land = src.at[c, peer, pl.ds(16 * part, 16)], dst.at[c, slot, pl.ds(16 * part, 16)]
             pltpu.make_async_remote_copy(
-                src_ref=src.at[c, peer], dst_ref=dst.at[c, slot], send_sem=send_sem.at[phase, c],
-                recv_sem=recv_sem.at[phase, c], device_id=device, device_id_type=MESH,
+                src_ref=send, dst_ref=land, send_sem=send_sem.at[phase, c], recv_sem=recv_sem.at[phase, c],
+                device_id=device, device_id_type=MESH,
             ).start()
-        dst[c, slot] = src[c, slot]
+        if part != 1:
+            dst[c, slot] = src[c, slot]
 
     def wait_all(sem, buf, c, count):
         span = buf.at[c, pl.ds(0, count - 1)]
@@ -115,12 +129,19 @@
                 for s in range(4):
                     t_buf[c, 4 * s + g] = res[32 * c : 32 * c + 32, 128 * s : 128 * s + 128]
 
-    def in_turn(c):
-        rhs = jnp.concatenate([w_buf[c, :, 16 * b : 16 * b + 16, :].reshape(256, 128) for b in range(2)], axis=1)
+    def turn(src, dst, c):
+        rhs = jnp.concatenate([src[c, :, 16 * b : 16 * b + 16, :].reshape(256, 128) for b in range(2)], axis=1)
         res = jnp.dot(in_flip_ref[...], rhs, preferred_element_type=F32).astype(BF16)
         for b in range(2):
             for i in range(16):
-                v_buf[c, 16 * b + i] = res[16 * i : 16 * i + 16, 128 * b : 128 * b + 128]
+                dst[c, 16 * b + i] = res[16 * i : 16 * i + 16, 128 * b : 128 * b + 128]
+
+    def turn_back(src, dst, c):
+        rhs = jnp.concatenate([src[c, 16 * b : 16 * b + 16].reshape(256, 128) for b in range(2)], axis=1)
+        res = jnp.dot(in_flip_ref[...], rhs, preferred_element_type=F32).astype(BF16)
+        for b in range(2):
+            for i in range(16):
+                dst[c, i, 16 * b : 16 * b + 16] = res[16 * i : 16 * i + 16, 128 * b : 128 * b + 128]
 
     def transform(c):
         f_buf[...] = jnp.dot(dft_ref[...], r_buf[c].reshape(512, 128), preferred_element_type=F32)
@@ -192,28 +213,43 @@
         with jax.named_scope(name):
             run(*args)
 
-    for load in loads[:5]:
+    for load in loads[:6]:
         load.wait()
     scope("channel", channel_transform)
+    scope("turn_x", turn, t_buf, v_buf, 0)
     with jax.named_scope("barrier"):
         pl.semaphore_wait(barrier, 46)
-    for c in range(4):
-        exchange(0, c, t_buf, w_buf, z_peer, z, FAR_FIRST)
-    for load in loads[5:]:
+    exchange(1, 0, v_buf, r_buf, rc_peer, me, RC_FAR_FIRST)
+    exchange(0, 1, t_buf, w_buf, z_peer, z, FAR_FIRST)
+    for load in loads[6:]:
         load.start()
-    for load in loads[5:]:
+    for load in loads[6:]:
         load.wait()
     scope("fuse_maps", fuse_maps)
 
+    def first_rc_in(c):
+        scope(f"wait_rc_in{c}", wait_all, recv_sem.at[1, c], r_buf, c, 32)
+        scope(f"turn_y{c}", turn_back, r_buf, t_buf, c)
+        exchange(0, 0, t_buf, w_buf, z_peer, z, FAR_FIRST)
+        exchange(0, 2, t_buf, w_buf, z_peer, z, FAR_FIRST)
+
+    def first_z_in(c):
+        scope(f"wait_z_in{c}", wait_all, recv_sem.at[0, c], w_buf, c, 16)
+        scope(f"turn_z{c}", turn, w_buf, r_buf, c)
+        scope(f"transform{c}", transform, c)
+        exchange(2, c, o_buf, m_buf, rc_peer, me, RC_FAR_FIRST)
+
     def z_in(c):
         scope(f"wait_z_in{c}", wait_all, recv_sem.at[0, c], w_buf, c, 16)
-        scope(f"in_turn{c}", in_turn, c)
-        exchange(1, c, v_buf, r_buf, rc_peer, me, range(1, 32))
+        scope(f"in_turn{c}", turn, w_buf, v_buf, c)
+        if c == 1:
+            exchange(0, 3, t_buf, w_buf, z_peer, z, FAR_FIRST)
+        exchange(1, c, v_buf, r_buf, rc_peer, me, RC_FAR_FIRST)
 
     def rc_in(c):
         scope(f"wait_rc_in{c}", wait_all, recv_sem.at[1, c], r_buf, c, 32)
         scope(f"transform{c}", transform, c)
-        exchange(2, c, o_buf, m_buf, rc_peer, me, range(1, 32))
+        exchange(2, c, o_buf, m_buf, rc_peer, me, RC_FAR_FIRST)
 
     def rc_out(c):
         scope(f"wait_rc_out{c}", wait_all, recv_sem.at[2, c], m_buf, c, 32)
@@ -221,8 +257,8 @@
         exchange(3, c, j_buf, s_buf, z_peer, z, FAR_FIRST)
 
     order = (
-        (z_in, 0), (z_in, 1), (rc_in, 0), (z_in, 2), (rc_in, 1), (rc_out, 0), (z_in, 3), (rc_in, 2), (rc_out, 1),
-        (rc_in, 3), (rc_out, 2), (rc_out, 3),
+        (first_rc_in, 0), (z_in, 1), (first_z_in, 0), (rc_in, 1), (z_in, 2), (rc_out, 0), (z_in, 3), (rc_out, 1),
+        (rc_in, 2), (rc_in, 3), (rc_out, 2), (rc_out, 3),
     )
     for stage, c in order:
         stage(c)

time: 68.9 us -> 67.6 us (0.981)
  Pallas kernels: 66.7 us -> 65.4 us
    pallas_call x1, Pallas kernels: 66.7 us -> 65.4 us  [per_device(): pl.pallas_call(mix_kernel, out_shape=[jax.ShapeDtypeStruct(shape, BF16) f...]
where the time goes in v5:
time: 67.6 us; the launch traced here: 67.4 us
  Pallas kernels  65.4 us (97%)
  matrix products  2.01 us (3%)
    pallas_call x1, Pallas kernels, per_device(): pl.pallas_call(mix_kernel, out_shape=[jax.ShapeDtypeStruct(shape, BF16) f...  65.4 us
    dot_general x1, matrix products, per_device(): jnp.dot(rows, late_map, preferred_element_type=F32) + part.astype(F32)  2.01 us

profile of v5, /device:TPU:1, one launch (start us, length us, event | category | flops | bytes accessed | tf_op | source)
XLA Modules:
  0.0 67.4 jit_solution(15525736248957497583)
XLA Ops:
  0.0 65.4 %shard_map.100 = (bf16[512,128]{1,0:T(8,128)(2,1)S(1)}, bf16[512,2048]{1,0:T(8,128)(2,1)S(1)}, bf16[128,2048]{1,0:T(8,128)(2,1)S(1)}) custom-call(bf16[4,128,512]{2,1,0:T(8,128)(2,1)} %x_hbm.1, bf16[128,128]{1,0:T(8,128)(2,1)} %constant.14.clone.chan_hbm, bf16[256,256]{1,0:T(8,128)(2,1)} %constant.15.clone.in_flip_hbm, ...), custom_call_target="tpu_custom_call" | custom-call | tf_op jit(solution)/shard_map/pallas_call | solution.py:285
  65.4 2.0 %add_convert_fusion = bf16[512,2048]{1,0:T(8,128)(2,1)} fusion(bf16[512,2048]{1,0:T(8,128)(2,1)S(1)} %get-tuple-element.10, bf16[512,128]{1,0:T(8,128)(2,1)S(1)} %get-tuple-element.8, bf16[128,2048]{1,0:T(8,128)(2,1)S(1)} %get-tuple-element.9), kind=kOutput, calls=%fused_computation | convolution fusion | flops 271581184 | bytes 4849664 | tf_op jit(solution)/shard_map/dot_general | solution.py:310

commit v6 on v5

--- a/solution.py
+++ b/solution.py
@@ -69,7 +69,7 @@
 def mix_kernel(
     x_hbm, chan_hbm, in_flip_hbm, dft_hbm, turn_hbm, last_hbm, out_flip_hbm, pick_hbm, group_hbm, out_map_hbm,
     rows_ref, part_ref, late_map_ref, x_ref, chan_ref, in_flip_ref, dft_ref, turn_ref, last_ref, out_flip_ref, pick_ref, group_ref, out_map_ref,
-    t_buf, w_buf, v_buf, r_buf, f_buf, g_buf, o_buf, m_buf, j_buf, s_buf, fused_buf, acc_buf, load_sem, send_sem, recv_sem,
+    t_buf, w_buf, v_buf, r_buf, g_buf, o_buf, m_buf, j_buf, s_buf, fused_buf, acc_buf, load_sem, send_sem, recv_sem,
 ):
     row = lax.axis_index("row")
     col = lax.axis_index("col")
@@ -144,17 +144,15 @@
                 dst[c, i, 16 * b : 16 * b + 16] = res[16 * i : 16 * i + 16, 128 * b : 128 * b + 128]
 
     def transform(c):
-        f_buf[...] = jnp.dot(dft_ref[...], r_buf[c].reshape(512, 128), preferred_element_type=F32)
-
-        def body(step, carry):
-            rows = pl.ds(pl.multiple_of(64 * step, 64), 64)
-            under = pl.ds(pl.multiple_of(512 + 64 * step, 64), 64)
-            re, im, cos, sin = f_buf[rows, :], f_buf[under, :], turn_ref[0, rows, :], turn_ref[1, rows, :]
+        rhs = r_buf[c].reshape(512, 128)
+
+        for step in range(2):
+            rows, under = pl.ds(256 * step, 256), pl.ds(512 + 256 * step, 256)
+            re = jnp.dot(dft_ref[rows, :], rhs, preferred_element_type=F32)
+            im = jnp.dot(dft_ref[under, :], rhs, preferred_element_type=F32)
+            cos, sin = turn_ref[0, rows, :], turn_ref[1, rows, :]
             g_buf[rows, 0:128] = (re * cos + im * sin).astype(BF16)
             g_buf[rows, 128:256] = (im * cos - re * sin).astype(BF16)
-            return carry
-
-        lax.fori_loop(0, 8, body, 0)
         kind = jnp.where(me == 0, 0, 1) if c == 1 else c % 2
         res = lax.dot_general(
             last_ref[kind], g_buf[...], (((1,), (1,)), ((), ())), preferred_element_type=F32
@@ -293,7 +291,6 @@
             pltpu.VMEM((4, 16, 32, 128), BF16),
             pltpu.VMEM((4, 32, 16, 128), BF16),
             pltpu.VMEM((4, 32, 16, 128), BF16),
-            pltpu.VMEM((1024, 128), F32),
             pltpu.VMEM((512, 256), BF16),
             pltpu.VMEM((4, 32, 2, 8, 128), BF16),
             pltpu.VMEM((4, 32, 2, 8, 128), BF16),

time: 67.6 us -> 66.4 us (0.982)
  Pallas kernels: 65.4 us -> 64.2 us
    pallas_call x1, Pallas kernels: 65.4 us -> 64.2 us  [per_device(): pl.pallas_call(mix_kernel, out_shape=[jax.ShapeDtypeStruct(shape, BF16) f...]
where the time goes in v6:
time: 66.4 us; the launch traced here: 66.3 us
  Pallas kernels  64.2 us (97%)
  matrix products  2.01 us (3%)
    pallas_call x1, Pallas kernels, per_device(): pl.pallas_call(mix_kernel, out_shape=[jax.ShapeDtypeStruct(shape, BF16) f...  64.2 us
    dot_general x1, matrix products, per_device(): jnp.dot(rows, late_map, preferred_element_type=F32) + part.astype(F32)  2.01 us

profile of v6, /device:TPU:1, one launch (start us, length us, event | category | flops | bytes accessed | tf_op | source)
XLA Modules:
  0.0 66.3 jit_solution(17055004544240906390)
XLA Ops:
  0.0 64.2 %shard_map.100 = (bf16[512,128]{1,0:T(8,128)(2,1)S(1)}, bf16[512,2048]{1,0:T(8,128)(2,1)S(1)}, bf16[128,2048]{1,0:T(8,128)(2,1)S(1)}) custom-call(bf16[4,128,512]{2,1,0:T(8,128)(2,1)} %x_hbm.1, bf16[128,128]{1,0:T(8,128)(2,1)} %constant.14.clone.chan_hbm, bf16[256,256]{1,0:T(8,128)(2,1)} %constant.15.clone.in_flip_hbm, ...), custom_call_target="tpu_custom_call" | custom-call | tf_op jit(solution)/shard_map/pallas_call | solution.py:283
  64.2 2.0 %add_convert_fusion = bf16[512,2048]{1,0:T(8,128)(2,1)} fusion(bf16[512,2048]{1,0:T(8,128)(2,1)S(1)} %get-tuple-element.10, bf16[512,128]{1,0:T(8,128)(2,1)S(1)} %get-tuple-element.8, bf16[128,2048]{1,0:T(8,128)(2,1)S(1)} %get-tuple-element.9), kind=kOutput, calls=%fused_computation | convolution fusion | flops 271581184 | bytes 4849664 | tf_op jit(solution)/shard_map/dot_general | solution.py:307

commit v7 on v6

--- a/solution.py
+++ b/solution.py
@@ -96,12 +96,16 @@
 
     barrier = pltpu.get_barrier_semaphore()
 
-    for step in FAR_FIRST:
-        pl.semaphore_signal(barrier, inc=1, device_id=z_peer(step)[1], device_id_type=MESH)
+    def greet(peer_of, steps):
+        for step in steps:
+            pl.semaphore_signal(barrier, inc=1, device_id=peer_of(step)[1], device_id_type=MESH)
+
+    greet(z_peer, FAR_FIRST[:9])
+    greet(rc_peer, RC_FAR_FIRST[:10])
     for load in loads[:6]:
         load.start()
-    for step in RC_FAR_FIRST:
-        pl.semaphore_signal(barrier, inc=1, device_id=rc_peer(step)[1], device_id_type=MESH)
+    greet(z_peer, FAR_FIRST[9:])
+    greet(rc_peer, RC_FAR_FIRST[10:])
 
     def exchange(phase, c, src, dst, peer_of, slot, order, part=None):
         for step in order:

time: 66.4 us -> 66.2 us (level)
  no operation moved by 1% of the time
where the time goes in v7:
time: 66.2 us; the launch traced here: 66.1 us
  Pallas kernels  64 us (97%)
  matrix products  2.02 us (3%)
    pallas_call x1, Pallas kernels, per_device(): pl.pallas_call(mix_kernel, out_shape=[jax.ShapeDtypeStruct(shape, BF16) f...  64 us
    dot_general x1, matrix products, per_device(): jnp.dot(rows, late_map, preferred_element_type=F32) + part.astype(F32)  2.02 us

profile of v7, /device:TPU:1, one launch (start us, length us, event | category | flops | bytes accessed | tf_op | source)
XLA Modules:
  0.0 66.1 jit_solution(13480882899916978929)
XLA Ops:
  0.0 64.0 %shard_map.100 = (bf16[512,128]{1,0:T(8,128)(2,1)S(1)}, bf16[512,2048]{1,0:T(8,128)(2,1)S(1)}, bf16[128,2048]{1,0:T(8,128)(2,1)S(1)}) custom-call(bf16[4,128,512]{2,1,0:T(8,128)(2,1)} %x_hbm.1, bf16[128,128]{1,0:T(8,128)(2,1)} %constant.14.clone.chan_hbm, bf16[256,256]{1,0:T(8,128)(2,1)} %constant.15.clone.in_flip_hbm, ...), custom_call_target="tpu_custom_call" | custom-call | tf_op jit(solution)/shard_map/pallas_call | solution.py:287
  64.1 2.0 %add_convert_fusion = bf16[512,2048]{1,0:T(8,128)(2,1)} fusion(bf16[512,2048]{1,0:T(8,128)(2,1)S(1)} %get-tuple-element.10, bf16[512,128]{1,0:T(8,128)(2,1)S(1)} %get-tuple-element.8, bf16[128,2048]{1,0:T(8,128)(2,1)S(1)} %get-tuple-element.9), kind=kOutput, calls=%fused_computation | convolution fusion | flops 271581184 | bytes 4849664 | tf_op jit(solution)/shard_map/dot_general | solution.py:311
